TPU v7x, 32 devices: a whole 2x2x4 slice. The times are simulated.
32 devices in a mesh: ep: 8 (over z, x), tp: 4 (over y, core).
Axes of the slice: x: 2, y: 2, z: 4, core: 2. Of those that a mesh axis runs over, the one named last changes fastest.
Arguments:
- x_in: bfloat16 [4096, 3072], P('tp', 'ep'), may hold values from -6 to 6
- z_in: bfloat16 [4096, 3072], P('tp', 'ep'), may hold values from -6 to 6
- dt_raw: float32 [64, 3072], P('tp', 'ep'), may hold values from -6 to 6
- decay_rate: float32 [64], P('tp'), may hold values from 0 to 1, as said below
- b_in: bfloat16 [256, 3072], P(None, 'ep'), may hold values from -6 to 6
- c_in: bfloat16 [256, 3072], P(None, 'ep'), may hold values from -6 to 6
- conv_x: float32 [4096, 4], P('tp'), may hold values from -3 to 3
- conv_b: float32 [256, 4], replicated, may hold values from -3 to 3
- conv_c: float32 [256, 4], replicated, may hold values from -3 to 3
- head_gain: float32 [4096], P('tp'), may hold values from 0.1 to 1.9
- moe_rows: bfloat16 [1280, 2048], P('ep'), may hold values from -6 to 6
- moe_gain: float32 [2048], replicated, may hold values from 0.1 to 1.9
- routes: int32 [1280, 2], P('ep'), may hold values from 0 to 7, all different within a row; in each aligned block of 160 rows (0 to 159, 160 to 319, ...) at most 80 rows name the same one
- route_logit: float32 [1280, 2], P('ep'), may hold values from -6 to 6
- w_gate: bfloat16 [8, 2048, 5120], P('ep', None, 'tp'), may hold values from -0.125 to 0.125
- w_up: bfloat16 [8, 2048, 5120], P('ep', None, 'tp'), may hold values from -0.125 to 0.125
- w_down: bfloat16 [8, 5120, 2048], P('ep', 'tp'), may hold values from -0.078125 to 0.078125
Outputs:
- mixed: bfloat16 [4096, 3072], P('tp', 'ep')
- moe_out: bfloat16 [2048, 1280], P('tp', 'ep')
Inputs may be any that keep to these rules, and one draw needn't show every extreme that they name: `routes`: each row names 2 different experts; among the rows of one index of ep no expert is named more than 80 times, a bound that some block reaches. `decay_rate`: positive rates.
All inputs are finite; a program needn't handle non-finite values.
Results may differ from a plain program's by a relative error of at most 0.018.
Values may be sent and summed in bfloat16 or wider, within the bound.
No kernel may reach another device: no remote copies, remote signals or barrier semaphores. Data moves between devices by JAX's collectives and lax.ppermute only.
A program may use at most 64 MiB of HBM per device.

v0:
```python
import jax
import jax.numpy as jnp
from jax import lax
from jax.experimental import pallas as pl
from jax.experimental.pallas import tpu as pltpu
from jax.sharding import PartitionSpec as P


HEAD_DIM = 64
GROUPS = 2
NSTATE = 128
BLOCK = 128
ROW_EPS = 0.1
HEAD_EPS = 1.0

BF = jnp.bfloat16
F32 = jnp.float32


def sds(shape, dtype):
    return jax.ShapeDtypeStruct(shape, dtype)


def whole(shape):
    return pl.BlockSpec(shape, lambda *a: (0,) * len(shape))


def dot(a, b):
    return jnp.dot(a, b, preferred_element_type=F32)


def silu(v):
    return v * (0.5 + 0.5 * jnp.tanh(0.5 * v))


def call(body, name, ids, *args, **kwargs):
    return launch(body, name, ids, *args, **kwargs)


def launch(body, name, ids, ins, outs, grid=None, in_specs=None, out_specs=None, scratch=(), us=1.0, mib=6):
    vmem = pl.BlockSpec(memory_space=pltpu.VMEM)
    common = dict(
        name=name,
        out_shape=outs,
        cost_estimate=pl.CostEstimate(
            flops=int(us * 2.5e8), bytes_accessed=0, transcendentals=0
        ),
    )
    limit = mib * 1024 * 1024
    if grid is None:
        return pl.pallas_call(
            body,
            in_specs=[pl.BlockSpec(memory_space=pltpu.SMEM)] + (in_specs or [vmem] * len(ins)),
            out_specs=out_specs or [vmem] * len(outs),
            scratch_shapes=list(scratch),
            compiler_params=pltpu.CompilerParams(vmem_limit_bytes=limit),
            **common,
        )(ids, *ins)
    return pl.pallas_call(
        body,
        grid_spec=pltpu.PrefetchScalarGridSpec(
            num_scalar_prefetch=1,
            grid=grid,
            in_specs=in_specs,
            out_specs=out_specs,
            scratch_shapes=list(scratch),
        ),
        compiler_params=pltpu.CompilerParams(
            dimension_semantics=("arbitrary",) * len(grid), vmem_limit_bytes=limit
        ),
        **common,
    )(ids, *ins)


GATE_MIB = 24
DOWN_MIB = 16
OPEN_MIB = 28


def in_hbm(value):
    return pltpu.with_memory_space_constraint(value, pltpu.HBM)


def ids_of(ids_ref):
    place, column = ids_ref[0], ids_ref[1]
    return place, column // 2, column % 2


def fill_rows(rows, count=8):
    width = rows[0].shape[1]
    at = lax.broadcasted_iota(jnp.int32, (count, width), 0)
    out = jnp.broadcast_to(rows[0], (count, width))
    for index in range(1, len(rows)):
        out = jnp.where(at == index, rows[index], out)
    return out


def destinations(routes_t, place, experts, capacity):
    tokens = routes_t.shape[1]
    relative = jnp.bitwise_xor(routes_t, place)
    first, second = relative[0:1, :], relative[1:2, :]
    at = lax.broadcasted_iota(jnp.int32, (experts, tokens), 0)
    hit_a = (at == first).astype(F32)
    hit_b = (at == second).astype(F32)
    row = lax.broadcasted_iota(jnp.int32, (tokens, tokens), 0)
    col = lax.broadcasted_iota(jnp.int32, (tokens, tokens), 1)
    before = (row < col).astype(F32).astype(BF)
    ahead = dot((hit_a + hit_b).astype(BF), before)
    rank_a = jnp.sum(hit_a * ahead, axis=0, keepdims=True).astype(jnp.int32)
    rank_b = jnp.sum(hit_b * ahead, axis=0, keepdims=True).astype(jnp.int32)
    return first * capacity + rank_a, second * capacity + rank_b


def prep(ids, moe_rows, moe_gain, routes_t, logit_t, x_in, b_in, c_in, sizes):
    tokens, features = moe_rows.shape
    experts, cap, width, y_count = sizes
    half = experts // 2
    value_rows, length = x_in.shape
    group_rows = b_in.shape[0] // GROUPS

    def body(ids_ref, rows_hbm, gain_hbm, routes_hbm, logit_hbm, x_hbm, b_hbm, c_hbm, *refs):
        outs, scratch = refs[:-9], refs[-9:]
        normed_ref, sems = scratch[0], scratch[-1]
        rows_ref, gain_ref, routes_ref, logit_ref, x_ref, b_ref, c_ref = scratch[1:-1]
        self_ref, near, far = outs[0], outs[1:half], outs[half : 2 * half]
        table_ref, rim_ref = outs[-2:]
        place, y, core = ids_of(ids_ref)
        tail = (slice(None), slice(length - 128, length))
        moves = (
            (rows_hbm, rows_ref),
            (gain_hbm, gain_ref),
            (routes_hbm, routes_ref),
            (logit_hbm, logit_ref),
            (x_hbm.at[tail], x_ref),
            (b_hbm.at[tail], b_ref),
            (c_hbm.at[tail], c_ref),
        )
        copies = [
            pltpu.make_async_copy(source, target, sems.at[index])
            for index, (source, target) in enumerate(moves)
        ]
        for copy in copies:
            copy.start()
        for copy in copies:
            copy.wait()
        rows = rows_ref[...].astype(F32)
        scale = lax.rsqrt(jnp.mean(rows * rows, axis=1, keepdims=True) + ROW_EPS)
        normed_ref[...] = (rows * scale * gain_ref[...]).astype(BF)
        dest_a, dest_b = destinations(routes_ref[...], place, experts, cap)

        def pick(index):
            slot = lax.broadcasted_iota(jnp.int32, (cap, tokens), 0) + index * cap
            return ((slot == dest_a) | (slot == dest_b)).astype(F32).astype(BF)

        def columns(block):
            return normed_ref[:, pl.ds(pl.multiple_of(block * width, width), width)]

        mine = columns(2 * y + core)
        for index in range(half):
            far[index][...] = dot(pick(half + index), mine).astype(BF)
        for j in range(y_count):
            part = columns(2 * j + core)
            for index in range(1, half):
                near[index - 1][:, j * width : (j + 1) * width] = dot(pick(index), part).astype(BF)
        self_ref[...] = dot(pick(0), normed_ref[...]).astype(BF)
        gap = logit_ref[0:1, :] - logit_ref[1:2, :]
        shares = [jax.nn.sigmoid(gap), jax.nn.sigmoid(-gap)]
        table_ref[...] = jnp.transpose(
            fill_rows([dest_a.astype(F32), dest_b.astype(F32)] + shares)
        )
        group = y * (GROUPS * 2) // (2 * y_count)
        start = pl.multiple_of(group * group_rows, group_rows)
        tail = lax.broadcasted_iota(jnp.int32, (16, 128), 0)
        lane = lax.broadcasted_iota(jnp.int32, (16, 128), 1)
        take = (lane == tail + 125).astype(F32).astype(BF)
        nt = (((1,), (1,)), ((), ()))

        def edge(block):
            return lax.dot_general(take, block, nt, preferred_element_type=F32).astype(BF)

        rim_ref[:, :value_rows] = edge(x_ref[...])
        rim_ref[:, value_rows : value_rows + group_rows] = edge(b_ref[pl.ds(start, group_rows), :])
        rim_ref[:, value_rows + group_rows :] = edge(c_ref[pl.ds(start, group_rows), :])

    outs = [sds((cap, features), BF)]
    outs += [sds((cap, y_count * width), BF)] * (half - 1)
    outs += [sds((cap, width), BF)] * half
    outs += [sds((tokens, 8), F32), sds((16, value_rows + 2 * group_rows), BF)]
    return call(
        body,
        "prep",
        ids,
        tuple(map(in_hbm, (moe_rows, moe_gain, routes_t, logit_t, x_in, b_in, c_in))),
        outs,
        in_specs=[pl.BlockSpec(memory_space=pltpu.HBM)] * 7,
        scratch=[
            pltpu.VMEM((tokens, features), BF),
            pltpu.VMEM(moe_rows.shape, BF),
            pltpu.VMEM(moe_gain.shape, F32),
            pltpu.VMEM(routes_t.shape, jnp.int32),
            pltpu.VMEM(logit_t.shape, F32),
            pltpu.VMEM((value_rows, 128), BF),
            pltpu.VMEM((b_in.shape[0], 128), BF),
            pltpu.VMEM((c_in.shape[0], 128), BF),
            pltpu.SemaphoreType.DMA((7,)),
        ],
        us=3.0,
        mib=10,
    )


def gate_up(ids, self_rows, near, near_other, far, far_other, w_gate, w_up, w_down, sizes):
    experts, cap, width, y_count = sizes
    features, hidden = w_gate.shape[1:]
    rows = experts * cap
    split = experts // 2 * cap
    step = 256 if hidden % 256 == 0 else hidden
    groups = (near, near_other, *far, *far_other)
    pieces = (self_rows, *(value for group in groups for value in group))

    def body(ids_ref, *refs):
        wg_ref, wu_ref, wd_ref, low_ref, high_ref, held_ref, lhs_ref, sem = refs[len(pieces) :]
        copy = pltpu.make_async_copy(wd_ref, held_ref, sem)
        copy.start()
        at, held = 1, []
        for group in groups:
            held.append(refs[at : at + len(group)])
            at += len(group)
        _, y, core = ids_of(ids_ref)

        def columns(block):
            return pl.ds(pl.multiple_of(block * width, width), width)

        lhs_ref[0:cap, :] = refs[0][...]
        for source, c in ((held[0], core), (held[1], 1 - core)):
            for index, ref in enumerate(source):
                lines = slice(cap * (1 + index), cap * (2 + index))
                for j in range(y_count):
                    lhs_ref[lines, columns(2 * j + c)] = ref[:, j * width : (j + 1) * width]
        for set_at, c in ((2, core), (2 + len(far), 1 - core)):
            start = split
            for source in held[set_at : set_at + len(far)]:
                tall_rows = source[0].shape[0]
                for j, ref in enumerate(source):
                    lines = slice(start, start + tall_rows)
                    lhs_ref[lines, columns(2 * jnp.bitwise_xor(y, j) + c)] = ref[...]
                start += tall_rows

        for turn in range(hidden // step):
            span = slice(turn * step, (turn + 1) * step)
            for lines, out_ref in ((slice(0, split), low_ref), (slice(split, rows), high_ref)):
                lhs = lhs_ref[lines, :]
                gate = dot(lhs, wg_ref[0, :, span])
                up = dot(lhs, wu_ref[0, :, span])
                out_ref[:, span] = (silu(gate) * up).astype(BF)
        copy.wait()

    vmem = pl.BlockSpec(memory_space=pltpu.VMEM)
    return call(
        body,
        "gate_up",
        ids,
        (*pieces, w_gate, w_up, in_hbm(w_down)),
        [sds((split, hidden), BF)] * 2 + [sds(w_down.shape, w_down.dtype)],
        in_specs=[vmem] * (len(pieces) + 2) + [pl.BlockSpec(memory_space=pltpu.HBM)],
        scratch=[pltpu.VMEM((rows, features), BF), pltpu.SemaphoreType.DMA],
        us=9.0,
        mib=GATE_MIB,
    )


def down(ids, hidden, w_down, sizes, name):
    _, _, width, y_count = sizes
    rows, _ = hidden.shape

    def body(ids_ref, h_ref, w_ref, send_ref, keep_ref):
        core = ids_ref[1] % 2
        for out_ref, c in ((send_ref, 1 - core), (keep_ref, core)):
            for j in range(y_count):
                column = pl.ds(pl.multiple_of((2 * j + c) * width, width), width)
                value = dot(h_ref[...], w_ref[0, :, column])
                out_ref[:, j * width : (j + 1) * width] = value.astype(BF)

    return call(
        body,
        name,
        ids,
        (hidden, w_down),
        [sds((rows, y_count * width), BF)] * 2,
        us=2.0,
        mib=DOWN_MIB,
    )


def near_sum(ids, keep, received, sizes):
    experts, cap, width, y_count = sizes
    half = experts // 2

    def body(ids_ref, keep_ref, recv_ref, *outs):
        for index in range(half):
            span = pl.ds(index * cap, cap)
            outs[index][...] = (
                keep_ref[span, :].astype(F32) + recv_ref[span, :].astype(F32)
            ).astype(BF)

    outs = [sds((cap, y_count * width), BF)] * half
    return call(body, "near_sum", ids, (keep, received), outs)


def far_split(ids, keep, received, sizes):
    _, _, width, y_count = sizes
    rows = keep.shape[0]

    def body(ids_ref, keep_ref, recv_ref, *outs):
        _, y, _ = ids_of(ids_ref)
        for part in range(2):
            lines = pl.ds(part * rows // 2, rows // 2)
            for j in range(y_count):
                column = pl.ds(pl.multiple_of(jnp.bitwise_xor(y, j) * width, width), width)
                outs[part * y_count + j][...] = (
                    keep_ref[lines, column].astype(F32) + recv_ref[lines, column].astype(F32)
                ).astype(BF)

    outs = [sds((rows // 2, width), BF)] * (2 * y_count)
    return call(body, "far_split", ids, (keep, received), outs)


def far_sum(ids, parts, sizes, name):
    experts, cap, width, _ = sizes
    count = experts // 4

    def body(ids_ref, *refs):
        ins, outs = refs[: len(parts)], refs[len(parts) :]
        for index in range(count):
            span = pl.ds(index * cap, cap)
            total = ins[0][span, :].astype(F32)
            for ref in ins[1:]:
                total = total + ref[span, :].astype(F32)
            outs[index][...] = total.astype(BF)

    return call(body, name, ids, parts, [sds((cap, width), BF)] * count)


def token_weights(table, cap):
    tokens = table.shape[0]
    first, second = table[:, 0:1], table[:, 1:2]
    share_a, share_b = table[:, 2:3], table[:, 3:4]

    def pick(index):
        slot = (lax.broadcasted_iota(jnp.int32, (tokens, cap), 1) + index * cap).astype(F32)
        return (
            jnp.where(slot == first, share_a, 0.0) + jnp.where(slot == second, share_b, 0.0)
        ).astype(BF)

    return pick


def near_combine(ids, parts, table, sizes):
    _, cap, width, y_count = sizes
    tokens = table.shape[0]

    def body(ids_ref, table_ref, *refs):
        ins, outs = refs[: len(parts)], refs[len(parts) :]
        _, y, _ = ids_of(ids_ref)
        pick = token_weights(table_ref[...], cap)
        picks = [pick(index) for index in range(len(parts))]
        for j in range(y_count):
            column = pl.ds(pl.multiple_of(jnp.bitwise_xor(y, j) * width, width), width)
            total = dot(picks[0], ins[0][:, column])
            for index in range(1, len(parts)):
                total = total + dot(picks[index], ins[index][:, column])
            outs[j][...] = total.astype(outs[j].dtype)

    outs = [sds((tokens, width), F32)] + [sds((tokens, width), BF)] * (y_count - 1)
    return call(body, "near_combine", ids, (table, *parts), outs)


def final_combine(ids, parts, near_keep, near_received, table, sizes):
    experts, cap, width, y_count = sizes
    tokens = table.shape[0]
    half = experts // 2

    def body(ids_ref, table_ref, keep_ref, *refs):
        received, ins, out_ref = refs[: y_count - 1], refs[y_count - 1 : -1], refs[-1]
        pick = token_weights(table_ref[...], cap)
        total = keep_ref[...]
        for ref in received:
            total = total + ref[...].astype(F32)
        for index in range(half):
            total = total + dot(pick(half + index), ins[index][...])
        out_ref[...] = total.astype(BF)

    return call(
        body,
        "final_combine",
        ids,
        (table, near_keep, *near_received, *parts),
        [sds((tokens, width), BF)],
    )[0]


def swap(value, axis, step):
    count = lax.axis_size(axis)
    return lax.ppermute(value, axis, [(i, i ^ step) for i in range(count)])


def tall(rows):
    return jnp.transpose(fill_rows(rows))


def conv_block(signal, rim_t, taps_t):
    kinds = [taps_t[k : k + 1, :] for k in range(taps_t.shape[0])]
    taps = tall(kinds)
    count = len(kinds)
    place = lax.broadcasted_iota(jnp.int32, (16, 128), 0)
    lane = lax.broadcasted_iota(jnp.int32, (16, 128), 1)
    put = ((lane == place + 125) & (place < 3)).astype(F32).astype(BF)
    edge = dot(jnp.transpose(rim_t.astype(F32)).astype(BF), put)
    value = signal.astype(F32)
    joined = jnp.concatenate([edge, value], axis=1)
    total = taps[:, count - 1 : count] * value
    for back in range(1, count):
        total = total + taps[:, count - 1 - back : count - back] * pltpu.roll(joined, back, 1)[:, 128:]
    return silu(total)


def head_rows(table, heads_here, length):
    return jnp.concatenate(
        [jnp.broadcast_to(table[i : i + 1, :], (HEAD_DIM, length)) for i in range(heads_here)], axis=0
    )


def mixer_open(ids, x_in, dt_raw, rate_row, b_in, c_in, taps_x, taps_b, taps_c, rims, weights, hb, hp, y_count):
    rows, length = x_in.shape
    heads = dt_raw.shape[0]
    block_rows = hb * HEAD_DIM

    def body(ids_ref, x_ref, dt_ref, rate_ref, b_ref, c_ref, tx_ref, tb_ref, tc_ref, rim_ref, *refs):
        from_refs, outs = refs[: len(weights)], refs[len(weights) :]
        xs_ref, cum_ref, bt_ref, conv_c_ref, msg_ref = outs[:5]
        into_refs, (step_ref, sems) = outs[5:-2], outs[-2:]
        copies = [
            pltpu.make_async_copy(source, target, sems.at[index])
            for index, (source, target) in enumerate(zip(from_refs, into_refs))
        ]
        _, y, _ = ids_of(ids_ref)
        turn = pl.program_id(0)

        @pl.when(turn == 0)
        def _():
            for copy in copies:
                copy.start()
            group = y * (GROUPS * 2) // (2 * y_count)
            start = pl.multiple_of(group * NSTATE, NSTATE)
            span = pl.ds(start, NSTATE)
            b_conv = conv_block(b_ref[span, :], rim_ref[:, rows : rows + NSTATE], tb_ref[:, span])
            c_conv = conv_block(c_ref[span, :], rim_ref[:, rows + NSTATE :], tc_ref[:, span])
            bt_ref[...] = jnp.transpose(b_conv).astype(BF)
            conv_c_ref[...] = c_conv.astype(BF)
            raw = dt_ref[...]
            step = jnp.maximum(raw, 0.0) + jnp.log1p(jnp.exp(-jnp.abs(raw)))
            eye_r = lax.broadcasted_iota(jnp.int32, (heads, heads), 0)
            eye_c = lax.broadcasted_iota(jnp.int32, (heads, heads), 1)
            rate = jnp.sum(jnp.where(eye_r == eye_c, rate_ref[...], 0.0), axis=1, keepdims=True)
            cum = -step * rate
            lane = lax.broadcasted_iota(jnp.int32, (heads, length), 1)
            shift = 1
            while shift < length:
                cum = cum + jnp.where(lane >= shift, pltpu.roll(cum, shift, 1), 0.0)
                shift *= 2
            step_ref[...] = step
            cum_ref[...] = cum
            total = jnp.broadcast_to(jnp.exp(cum[:, length - 1 : length]), (heads, NSTATE))
            if heads < hp:
                total = jnp.concatenate([total, jnp.ones((hp - heads, NSTATE), F32)], axis=0)
            high = total.astype(BF)
            msg_ref[rows : rows + hp, :] = high
            msg_ref[rows + hp : rows + 2 * hp, :] = (total - high.astype(F32)).astype(BF)

        value = conv_block(x_ref[...], rim_ref[:, pl.ds(pl.multiple_of(turn * block_rows, block_rows), block_rows)], tx_ref[...])
        first = turn * hb if heads > hb else 0
        step = step_ref[pl.ds(first, hb), :]
        cum = cum_ref[pl.ds(first, hb), :]
        fade = jnp.exp(cum[:, length - 1 : length] - cum)
        scaled = value * head_rows(step, hb, length)
        xs_ref[...] = scaled.astype(BF)
        state = dot((scaled * head_rows(fade, hb, length)).astype(BF), bt_ref[...])
        msg_ref[pl.ds(pl.multiple_of(turn * block_rows, block_rows), block_rows), :] = state.astype(BF)

        @pl.when(turn == heads // hb - 1)
        def _():
            for copy in copies:
                copy.wait()

    outs = [
        sds((rows, length), BF),
        sds((heads, length), F32),
        sds((length, NSTATE), BF),
        sds((NSTATE, length), BF),
        sds((rows + 2 * hp, NSTATE), BF),
    ] + [sds(w.shape, w.dtype) for w in weights]
    vmem = pl.BlockSpec(memory_space=pltpu.VMEM)
    return call(
        body,
        "mixer_open",
        ids,
        (*map(in_hbm, (x_in, dt_raw, rate_row, b_in, c_in, taps_x, taps_b, taps_c)), rims, *map(in_hbm, weights)),
        outs,
        grid=(heads // hb,),
        in_specs=[
            pl.BlockSpec((block_rows, length), lambda i, s: (i, 0)),
            whole(dt_raw.shape),
            whole(rate_row.shape),
            whole(b_in.shape),
            whole(c_in.shape),
            pl.BlockSpec((taps_x.shape[0], block_rows), lambda i, s: (0, i)),
            whole(taps_b.shape),
            whole(taps_c.shape),
            vmem,
        ]
        + [pl.BlockSpec(memory_space=pltpu.HBM)] * len(weights),
        out_specs=[pl.BlockSpec((block_rows, length), lambda i, s: (i, 0))]
        + [whole(o.shape) for o in outs[1:5]]
        + [vmem] * len(weights),
        scratch=[pltpu.VMEM((heads, length), F32), pltpu.SemaphoreType.DMA((len(weights),))],
        us=7.0,
        mib=OPEN_MIB,
    )


def per_row(table, heads):
    width = table.shape[1]
    return jnp.broadcast_to(table[:heads][:, None, :], (heads, HEAD_DIM, width)).reshape(
        heads * HEAD_DIM, width
    )


def state_round(ids, mine, received, carried, level, heads, hp):
    rows = heads * HEAD_DIM
    opening = carried is None
    outs = [sds(mine.shape, BF), sds((rows, NSTATE), F32), sds((hp, NSTATE), F32)]

    def body(ids_ref, mine_ref, recv_ref, *refs):
        msg_ref, pre_ref, dec_ref = refs[-3:]
        upper = (ids_ref[0] >> level) % 2 == 1
        t_mine = mine_ref[:rows, :].astype(F32)
        t_recv = recv_ref[:rows, :].astype(F32)

        def decay(ref):
            return ref[rows : rows + hp, :].astype(F32) + ref[rows + hp :, :].astype(F32)

        d_mine, d_recv = decay(mine_ref), decay(recv_ref)
        one = jnp.ones_like(d_mine)
        d_late = jnp.where(upper, d_mine, d_recv)
        late = jnp.where(upper, t_mine, t_recv)
        early = jnp.where(upper, t_recv, t_mine)
        total = late + per_row(d_late, heads) * early
        msg_ref[:rows, :] = total.astype(BF)
        both = d_mine * d_recv
        high = both.astype(BF)
        msg_ref[rows : rows + hp, :] = high
        msg_ref[rows + hp :, :] = (both - high.astype(F32)).astype(BF)
        if opening:
            pre_ref[...] = jnp.where(upper, t_recv, jnp.zeros_like(t_recv))
            dec_ref[...] = jnp.where(upper, d_recv, one)
        else:
            old_pre, old_dec = refs[0], refs[1]
            grown = old_pre[...] + per_row(old_dec[...], heads) * t_recv
            pre_ref[...] = jnp.where(upper, grown, old_pre[...])
            dec_ref[...] = jnp.where(upper, old_dec[...] * d_recv, old_dec[...])

    ins = (mine, received) if opening else (mine, received, *carried)
    return call(body, f"state_round_{level}", ids, ins, outs)


def mixer_close(ids, carried, received, xs, cum, b_t, c_conv, z_in, gain_row, hb):
    rows, length = xs.shape
    heads = cum.shape[0]
    block_rows = hb * HEAD_DIM
    blocks = length // BLOCK

    def body(ids_ref, pre_ref, dec_ref, recv_ref, xs_ref, cum_ref, bt_ref, c_ref, z_ref, gain_ref, out_ref, gram_ref, y_ref):
        turn = pl.program_id(0)

        @pl.when(turn == 0)
        def _():
            row = lax.broadcasted_iota(jnp.int32, (BLOCK, BLOCK), 0)
            col = lax.broadcasted_iota(jnp.int32, (BLOCK, BLOCK), 1)
            for j in range(blocks):
                span = slice(j * BLOCK, (j + 1) * BLOCK)
                gram = dot(bt_ref[span, :], c_ref[:, span])
                gram_ref[j] = jnp.where(row <= col, gram, 0.0)

        first = turn * hb if heads > hb else 0
        decay = dec_ref[pl.ds(first, hb), :]
        own = pl.ds(pl.multiple_of(turn * block_rows, block_rows), block_rows)
        state = pre_ref[own, :] + head_rows(decay, hb, NSTATE) * recv_ref[own, :].astype(F32)
        cum = cum_ref[...]
        down_cum = jnp.transpose(fill_rows([cum[i : i + 1, :] for i in range(hb)]))
        before = jnp.zeros((hb, 1), F32)
        for j in range(blocks):
            span = slice(j * BLOCK, (j + 1) * BLOCK)
            here = cum[:, span]
            after = here[:, BLOCK - 1 : BLOCK]
            c_block = c_ref[:, span]
            flow = dot(state.astype(BF), c_block) * head_rows(jnp.exp(here - before), hb, BLOCK)
            gram = gram_ref[j]
            for i in range(hb):
                lines = slice(i * HEAD_DIM, (i + 1) * HEAD_DIM)
                gap = jnp.minimum(here[i : i + 1, :] - down_cum[span, i : i + 1], 0.0)
                mask = (gram * jnp.exp(gap)).astype(BF)
                y_ref[lines, span] = flow[lines, :] + dot(xs_ref[lines, span], mask)
            if j + 1 < blocks:
                fade = head_rows(jnp.exp(after - here), hb, BLOCK)
                fresh = dot((xs_ref[:, span].astype(F32) * fade).astype(BF), bt_ref[span, :])
                kept = head_rows(jnp.broadcast_to(jnp.exp(after - before), (hb, NSTATE)), hb, NSTATE)
                state = kept * state + fresh
            before = after
        gain = tall([gain_ref[...]])
        for i in range(hb):
            lines = slice(i * HEAD_DIM, (i + 1) * HEAD_DIM)
            gated = y_ref[lines, :] * silu(z_ref[lines, :].astype(F32))
            scale = lax.rsqrt(jnp.mean(gated * gated, axis=0, keepdims=True) + HEAD_EPS)
            out_ref[lines, :] = (gated * scale * gain[lines, 0:1]).astype(BF)

    pre, dec = carried
    tile = pl.BlockSpec((block_rows, length), lambda i, s: (i, 0))
    vmem = pl.BlockSpec(memory_space=pltpu.VMEM)
    return call(
        body,
        "mixer_close",
        ids,
        (pre, dec, received, xs, cum, b_t, c_conv, in_hbm(z_in), in_hbm(gain_row)),
        [sds((rows, length), BF)],
        grid=(heads // hb,),
        in_specs=[
            vmem,
            vmem,
            vmem,
            tile,
            pl.BlockSpec((hb, length), lambda i, s: (i, 0)),
            whole(b_t.shape),
            whole(c_conv.shape),
            tile,
            pl.BlockSpec((1, block_rows), lambda i, s: (0, i)),
        ],
        out_specs=[tile],
        scratch=[pltpu.VMEM((blocks, BLOCK, BLOCK), F32), pltpu.VMEM((block_rows, length), F32)],
        us=6.0,
        mib=12,
    )[0]


def block(
    x_in,
    z_in,
    dt_raw,
    decay_rate,
    b_in,
    c_in,
    conv_x,
    conv_b,
    conv_c,
    head_gain,
    moe_rows,
    moe_gain,
    routes,
    route_logit,
    w_gate,
    w_up,
    w_down,
):
    ep, tp = lax.axis_size("ep"), lax.axis_size("tp")
    y_count = tp // 2
    heads = dt_raw.shape[0]
    hb, hp = min(8, heads), -(-heads // 16) * 16
    tokens, features = moe_rows.shape
    experts = ep * w_gate.shape[0]
    capacity = 2 * tokens * routes.shape[1] // experts
    cap = -(-capacity // 16) * 16
    sizes = (experts, cap, features // tp, y_count)
    half = experts // 2
    ids = jnp.stack([lax.axis_index("ep"), lax.axis_index("tp")]).astype(jnp.int32)
    routes_t, logit_t = routes.T, route_logit.T

    outs = prep(ids, moe_rows, moe_gain.reshape(1, -1), routes_t, logit_t, x_in, b_in, c_in, sizes)
    self_rows, near, far = outs[0], outs[1:half], outs[half : 2 * half]
    table, own_rims = outs[-2:]
    rims = lax.ppermute(own_rims, "ep", [(i, i + 1) for i in range(ep - 1)])
    far = [swap(value, "ep", half + index) for index, value in enumerate(far)]
    near = [swap(value, "ep", 1 + index) for index, value in enumerate(near)]
    far_sets = []
    for part in range(2):
        mine = far[part * half // 2 : (part + 1) * half // 2]
        value = jnp.concatenate(mine, axis=0)
        far_sets.append([value] + [swap(value, "tp", 2 * j) for j in range(1, y_count)])
    near_other = [swap(value, "tp", 1) for value in near]
    far_other = [[swap(value, "tp", 1) for value in group] for group in far_sets]

    xs, cum, b_t, c_conv, message, w_gate, w_up = mixer_open(
        ids,
        x_in,
        dt_raw,
        decay_rate.reshape(1, -1),
        b_in,
        c_in,
        conv_x.T,
        conv_b.T,
        conv_c.T,
        rims,
        (w_gate, w_up),
        hb,
        hp,
        y_count,
    )
    carried, level = None, 0
    while (2 << level) < ep:
        received = swap(message, "ep", 1 << level)
        message, *carried = state_round(ids, message, received, carried, level, heads, hp)
        level += 1
    top = 1 << level
    last = lax.ppermute(message, "ep", [(i, i + top) for i in range(ep - top)])

    hid_near, hid_far, w_down = gate_up(
        ids, self_rows, near, near_other, far_sets, far_other, w_gate, w_up, w_down, sizes
    )
    send_far, keep_far = down(ids, hid_far, w_down, sizes, "down_far")
    recv_far = swap(send_far, "tp", 1)
    send_near, keep_near = down(ids, hid_near, w_down, sizes, "down_near")
    recv_near = swap(send_near, "tp", 1)
    near_out = near_sum(ids, keep_near, recv_near, sizes)
    near_back = [near_out[0]] + [swap(near_out[k], "ep", k) for k in range(1, half)]
    far_outs = far_split(ids, keep_far, recv_far, sizes)
    far_back = []
    for part in range(2):
        far_keep, *far_send = far_outs[part * y_count : (part + 1) * y_count]
        label = "ab"[part]
        far_parts = [far_keep] + [
            swap(value, "tp", 2 * (j + 1)) for j, value in enumerate(far_send)
        ]
        far_out = far_sum(ids, far_parts, sizes, "far_sum_" + label)
        first = half + part * (half // 2)
        far_back += [swap(value, "ep", first + index) for index, value in enumerate(far_out)]
    outs = near_combine(ids, near_back, table, sizes)
    near_keep = outs[0]
    near_received = [swap(value, "tp", 2 * (j + 1)) for j, value in enumerate(outs[1:])]
    moe_t = final_combine(ids, far_back, near_keep, near_received, table, sizes)

    mixed = mixer_close(
        ids, carried, last, xs, cum, b_t, c_conv, z_in, head_gain.reshape(1, -1), hb
    )
    return (mixed, moe_t.T)


def solution(mesh):
    return jax.shard_map(
        block,
        mesh=mesh,
        in_specs=(
            P("tp", "ep"),
            P("tp", "ep"),
            P("tp", "ep"),
            P("tp"),
            P(None, "ep"),
            P(None, "ep"),
            P("tp", None),
            P(),
            P(),
            P("tp"),
            P("ep", None),
            P(),
            P("ep", None),
            P("ep", None),
            P("ep", None, "tp"),
            P("ep", None, "tp"),
            P("ep", "tp", None),
        ),
        out_specs=(P("tp", "ep"), P("tp", "ep")),
        check_vma=False,
    )
```

profile of v0, /device:TPU:0, one launch (start us, length us, event | category | flops | bytes accessed | tf_op | source)
XLA Modules:
  0.0 109.8 jit_solution(7002642143872944995)
XLA Ops:
  0.7 2.7 %prep.1 = (bf16[80,2048]{1,0:T(8,128)(2,1)S(1)}, bf16[80,1024]{1,0:T(8,128)(2,1)S(1)}, bf16[80,1024]{1,0:T(8,128)(2,1)S(1)}, bf16[80,1024]{1,0:T(8,128)(2,1)S(1)...) custom-call(s32[2]{0:T(128)S(1)} %pad_add_fusion.ids_ref, ...), custom_call_target="tpu_custom_call" | custom-call | flops 750000000 | tf_op jit(solution)/shard_map/prep/pallas_call | solution.py:51
  3.4 4.1 %collective-permute-start.10 = (bf16[80,512]{1,0:T(8,128)(2,1)S(1)}, bf16[80,512]{1,0:T(8,128)(2,1)S(1)}, u32[]{:S(2)}, u32[]{:S(2)}) collective-permute-start(bf16[80,512]{1,0:T(8,128)(2,1)S(1)} %get-tuple-element.63), channel_id=1, source_target_pairs={{0,16},{4,20},{8,24},{12,28},{16,0},{20,4},{24,8},{28,12},{1,17},{... | collective-permute-start | bytes 245768 | tf_op jit(solution)/shard_map/ppermute | solution.py:404
  7.6 3.4 %collective-permute-start = (bf16[16,1280]{1,0:T(8,128)(2,1)S(1)}, bf16[16,1280]{1,0:T(8,128)(2,1)S(1)}, u32[]{:S(2)}, u32[]{:S(2)}) collective-permute-start(bf16[16,1280]{1,0:T(8,128)(2,1)S(1)} %get-tuple-element.46), channel_id=1, source_target_pairs={{0,4},{4,8},{8,12},{12,16},{16,20},{20,24},{24,28},{1,5},{5,9},{9,... | collective-permute-start | bytes 122888 | tf_op jit(solution)/shard_map/ppermute | solution.py:689
  11.0 1.4 %collective-permute-start.11 = (bf16[80,512]{1,0:T(8,128)(2,1)S(1)}, bf16[80,512]{1,0:T(8,128)(2,1)S(1)}, u32[]{:S(2)}, u32[]{:S(2)}) collective-permute-start(bf16[80,512]{1,0:T(8,128)(2,1)S(1)} %get-tuple-element.64), channel_id=1, source_target_pairs={{0,20},{4,16},{8,28},{12,24},{16,4},{20,0},{24,12},{28,8},{1,21},{... | collective-permute-start | bytes 245768 | tf_op jit(solution)/shard_map/ppermute | solution.py:404
  12.3 2.1 %collective-permute-start.13 = (bf16[80,512]{1,0:T(8,128)(2,1)S(1)}, bf16[80,512]{1,0:T(8,128)(2,1)S(1)}, u32[]{:S(2)}, u32[]{:S(2)}) collective-permute-start(bf16[80,512]{1,0:T(8,128)(2,1)S(1)} %get-tuple-element.65), channel_id=1, source_target_pairs={{0,24},{4,28},{8,16},{12,20},{16,8},{20,12},{24,0},{28,4},{1,25},{... | collective-permute-start | bytes 245768 | tf_op jit(solution)/shard_map/ppermute | solution.py:404
  14.4 1.7 %collective-permute-start.14 = (bf16[80,512]{1,0:T(8,128)(2,1)S(1)}, bf16[80,512]{1,0:T(8,128)(2,1)S(1)}, u32[]{:S(2)}, u32[]{:S(2)}) collective-permute-start(bf16[80,512]{1,0:T(8,128)(2,1)S(1)} %get-tuple-element.66), channel_id=1, source_target_pairs={{0,28},{4,24},{8,20},{12,16},{16,12},{20,8},{24,4},{28,0},{1,29},{... | collective-permute-start | bytes 245768 | tf_op jit(solution)/shard_map/ppermute | solution.py:404
  16.1 1.5 %collective-permute-start.4 = (bf16[80,1024]{1,0:T(8,128)(2,1)S(1)}, bf16[80,1024]{1,0:T(8,128)(2,1)S(1)}, u32[]{:S(2)}, u32[]{:S(2)}) collective-permute-start(bf16[80,1024]{1,0:T(8,128)(2,1)S(1)} %get-tuple-element.60), channel_id=1, source_target_pairs={{0,4},{4,0},{8,12},{12,8},{16,20},{20,16},{24,28},{28,24},{1,5},{5... | collective-permute-start | bytes 491528 | tf_op jit(solution)/shard_map/ppermute | solution.py:404
  18.6 5.6 %collective-permute-start.5 = (bf16[80,1024]{1,0:T(8,128)(2,1)S(1)}, bf16[80,1024]{1,0:T(8,128)(2,1)S(1)}, u32[]{:S(2)}, u32[]{:S(2)}) collective-permute-start(bf16[80,1024]{1,0:T(8,128)(2,1)S(1)} %get-tuple-element.61), channel_id=1, source_target_pairs={{0,8},{4,12},{8,0},{12,4},{16,24},{20,28},{24,16},{28,20},{1,9},{5... | collective-permute-start | bytes 491528 | tf_op jit(solution)/shard_map/ppermute | solution.py:404
  24.2 2.3 %collective-permute-start.6 = (bf16[80,1024]{1,0:T(8,128)(2,1)S(1)}, bf16[80,1024]{1,0:T(8,128)(2,1)S(1)}, u32[]{:S(2)}, u32[]{:S(2)}) collective-permute-start(bf16[80,1024]{1,0:T(8,128)(2,1)S(1)} %get-tuple-element.62), channel_id=1, source_target_pairs={{0,12},{4,8},{8,4},{12,0},{16,28},{20,24},{24,20},{28,16},{1,13},{... | collective-permute-start | bytes 491528 | tf_op jit(solution)/shard_map/ppermute | solution.py:404
  26.7 1.6 %collective-permute-start.15 = (bf16[160,512]{1,0:T(8,128)(2,1)S(1)}, bf16[160,512]{1,0:T(8,128)(2,1)S(1)}, u32[]{:S(2)}, u32[]{:S(2)}) collective-permute-start(bf16[160,512]{1,0:T(8,128)(2,1)S(1)} %constant_dynamic-update-slice_fusion.2.refs_9_), channel_id=1, source_target_pairs={{0,2},{1,3},{2,0},{3,1},{4,6},{5,7},{6,4},{7,5},{8,10},{9,11},{10,... | collective-permute-start | bytes 491528 | tf_op jit(solution)/shard_map/ppermute | solution.py:404
  29.2 1.5 %collective-permute-start.12 = (bf16[160,512]{1,0:T(8,128)(2,1)S(1)}, bf16[160,512]{1,0:T(8,128)(2,1)S(1)}, u32[]{:S(2)}, u32[]{:S(2)}) collective-permute-start(bf16[160,512]{1,0:T(8,128)(2,1)S(1)} %constant_dynamic-update-slice_fusion.refs_7_), channel_id=1, source_target_pairs={{0,2},{1,3},{2,0},{3,1},{4,6},{5,7},{6,4},{7,5},{8,10},{9,11},{10,... | collective-permute-start | bytes 491528 | tf_op jit(solution)/shard_map/ppermute | solution.py:404
  32.2 1.6 %collective-permute-done.15.refs_10_ = bf16[160,512]{1,0:T(8,128)(2,1)S(1)} collective-permute-done((bf16[160,512]{1,0:T(8,128)(2,1)S(1)}, bf16[160,512]{1,0:T(8,128)(2,1)S(1)}, u32[]{:S(2)}, u32[]{:S(2)}) %collective-permute-start.15) | collective-permute-done | bytes 163872 | tf_op jit(solution)/shard_map/ppermute | solution.py:404
  34.3 2.5 %collective-permute-done.12.refs_8_ = bf16[160,512]{1,0:T(8,128)(2,1)S(1)} collective-permute-done((bf16[160,512]{1,0:T(8,128)(2,1)S(1)}, bf16[160,512]{1,0:T(8,128)(2,1)S(1)}, u32[]{:S(2)}, u32[]{:S(2)}) %collective-permute-start.12) | collective-permute-done | bytes 163872 | tf_op jit(solution)/shard_map/ppermute | solution.py:404
  36.8 6.6 %mixer_open.1 = (bf16[1024,384]{1,0:T(8,128)(2,1)S(1)}, f32[16,384]{1,0:T(8,128)S(1)}, bf16[384,128]{1,0:T(8,128)(2,1)S(1)}, bf16[128,384]{1,0:T(8,128)(2,1)S(1)...) custom-call(s32[2]{0:T(128)S(1)} %pad_add_fusion.ids_ref, ...), custom_call_target="tpu_custom_call" | custom-call | flops 1750000000 | tf_op jit(solution)/shard_map/mixer_open/pallas_call | solution.py:59
  43.4 8.0 %gate_up.1 = (bf16[320,1280]{1,0:T(8,128)(2,1)S(1)}, bf16[320,1280]{1,0:T(8,128)(2,1)S(1)}, bf16[1,1280,2048]{2,1,0:T(8,128)(2,1)S(1)}) custom-call(s32[2]{0:T(128)S(1)} %pad_add_fusion.ids_ref, bf16[80,2048]{1,0:T(8,128)(2,1)S(1)} %get-tuple-element.59.refs_0_, bf16[80,1024]{1,0:T(8,128)(2,1)S(1)} %collective-permute-done.4.refs_1_, ...), custom_call_target="tpu_custom_call" | custom-call | flops 2249999872 | tf_op jit(solution)/shard_map/gate_up/pallas_call | solution.py:51
  51.5 2.4 %down_near.1 = (bf16[320,1024]{1,0:T(8,128)(2,1)S(1)}, bf16[320,1024]{1,0:T(8,128)(2,1)S(1)}) custom-call(s32[2]{0:T(128)S(1)} %pad_add_fusion.ids_ref, bf16[320,1280]{1,0:T(8,128)(2,1)S(1)} %get-tuple-element.69.h_ref, bf16[1,1280,2048]{2,1,0:T(8,128)(2,1)S(1)} %get-tuple-element.70.w_ref), custom_call_target="tpu_custom_call" | custom-call | flops 500000000 | tf_op jit(solution)/shard_map/down_near/pallas_call | solution.py:51
  54.5 2.4 %down_far.1 = (bf16[320,1024]{1,0:T(8,128)(2,1)S(1)}, bf16[320,1024]{1,0:T(8,128)(2,1)S(1)}) custom-call(s32[2]{0:T(128)S(1)} %pad_add_fusion.ids_ref, bf16[320,1280]{1,0:T(8,128)(2,1)S(1)} %get-tuple-element.79.h_ref, bf16[1,1280,2048]{2,1,0:T(8,128)(2,1)S(1)} %get-tuple-element.70.w_ref), custom_call_target="tpu_custom_call" | custom-call | flops 500000000 | tf_op jit(solution)/shard_map/down_far/pallas_call | solution.py:51
  57.8 8.1 %collective-permute-done.1.recv_ref = bf16[1056,128]{1,0:T(8,128)(2,1)S(1)} collective-permute-done((bf16[1056,128]{1,0:T(8,128)(2,1)S(1)}, bf16[1056,128]{1,0:T(8,128)(2,1)S(1)}, u32[]{:S(2)}, u32[]{:S(2)}) %collective-permute-start.1) | collective-permute-done | bytes 270368 | tf_op jit(solution)/shard_map/ppermute | solution.py:404
  68.7 6.0 %collective-permute-done.2.recv_ref = bf16[1056,128]{1,0:T(8,128)(2,1)S(1)} collective-permute-done((bf16[1056,128]{1,0:T(8,128)(2,1)S(1)}, bf16[1056,128]{1,0:T(8,128)(2,1)S(1)}, u32[]{:S(2)}, u32[]{:S(2)}) %collective-permute-start.2) | collective-permute-done | bytes 270368 | tf_op jit(solution)/shard_map/ppermute | solution.py:404
  75.4 2.9 %collective-permute-start.3 = (bf16[1056,128]{1,0:T(8,128)(2,1)S(1)}, bf16[1056,128]{1,0:T(8,128)(2,1)S(1)}, u32[]{:S(2)}, u32[]{:S(2)}) collective-permute-start(bf16[1056,128]{1,0:T(8,128)(2,1)S(1)} %get-tuple-element.53), channel_id=1, source_target_pairs={{0,16},{4,20},{8,24},{12,28},{1,17},{5,21},{9,25},{13,29},{2,18},{... | collective-permute-start | bytes 811016 | tf_op jit(solution)/shard_map/ppermute | solution.py:722
  78.3 1.5 %collective-permute-start.22 = (bf16[80,1024]{1,0:T(8,128)(2,1)S(1)}, bf16[80,1024]{1,0:T(8,128)(2,1)S(1)}, u32[]{:S(2)}, u32[]{:S(2)}) collective-permute-start(bf16[80,1024]{1,0:T(8,128)(2,1)S(1)} %get-tuple-element.75), channel_id=1, source_target_pairs={{0,8},{4,12},{8,0},{12,4},{16,24},{20,28},{24,16},{28,20},{1,9},{5... | collective-permute-start | bytes 491528 | tf_op jit(solution)/shard_map/ppermute | solution.py:404
  79.8 1.2 %collective-permute-start.23 = (bf16[80,1024]{1,0:T(8,128)(2,1)S(1)}, bf16[80,1024]{1,0:T(8,128)(2,1)S(1)}, u32[]{:S(2)}, u32[]{:S(2)}) collective-permute-start(bf16[80,1024]{1,0:T(8,128)(2,1)S(1)} %get-tuple-element.76), channel_id=1, source_target_pairs={{0,12},{4,8},{8,4},{12,0},{16,28},{20,24},{24,20},{28,16},{1,13},{... | collective-permute-start | bytes 491528 | tf_op jit(solution)/shard_map/ppermute | solution.py:404
  81.7 1.6 %collective-permute-start.26 = (bf16[160,512]{1,0:T(8,128)(2,1)S(1)}, bf16[160,512]{1,0:T(8,128)(2,1)S(1)}, u32[]{:S(2)}, u32[]{:S(2)}) collective-permute-start(bf16[160,512]{1,0:T(8,128)(2,1)S(1)} %get-tuple-element.83), channel_id=1, source_target_pairs={{0,2},{1,3},{2,0},{3,1},{4,6},{5,7},{6,4},{7,5},{8,10},{9,11},{10,... | collective-permute-start | bytes 491528 | tf_op jit(solution)/shard_map/ppermute | solution.py:404
  83.8 4.2 %collective-permute-done.22.refs_2_ = bf16[80,1024]{1,0:T(8,128)(2,1)S(1)} collective-permute-done((bf16[80,1024]{1,0:T(8,128)(2,1)S(1)}, bf16[80,1024]{1,0:T(8,128)(2,1)S(1)}, u32[]{:S(2)}, u32[]{:S(2)}) %collective-permute-start.22) | collective-permute-done | bytes 163872 | tf_op jit(solution)/shard_map/ppermute | solution.py:404
  88.0 1.8 %collective-permute-done.23.refs_3_ = bf16[80,1024]{1,0:T(8,128)(2,1)S(1)} collective-permute-done((bf16[80,1024]{1,0:T(8,128)(2,1)S(1)}, bf16[80,1024]{1,0:T(8,128)(2,1)S(1)}, u32[]{:S(2)}, u32[]{:S(2)}) %collective-permute-start.23) | collective-permute-done | bytes 163872 | tf_op jit(solution)/shard_map/ppermute | solution.py:404
  89.8 1.2 %near_combine.1 = (f32[160,512]{1,0:T(8,128)S(1)}, bf16[160,512]{1,0:T(8,128)(2,1)S(1)}) custom-call(s32[2]{0:T(128)S(1)} %pad_add_fusion.ids_ref, f32[160,8]{1,0:T(8,128)S(1)} %get-tuple-element.58.table_ref, bf16[80,1024]{1,0:T(8,128)(2,1)S(1)} %get-tuple-element.73.refs_0_, bf16[80,1024]{1,0:T(8,128)(2,1)S(1)} %collective-permute-done.21.refs_1_, ...), custom_call_target="tpu_custom_call" | custom-call | flops 250000000 | tf_op jit(solution)/shard_map/near_combine/pallas_call | solution.py:51
  90.9 1.6 %collective-permute-start.24 = (bf16[160,512]{1,0:T(8,128)(2,1)S(1)}, bf16[160,512]{1,0:T(8,128)(2,1)S(1)}, u32[]{:S(2)}, u32[]{:S(2)}) collective-permute-start(bf16[160,512]{1,0:T(8,128)(2,1)S(1)} %get-tuple-element.78), channel_id=1, source_target_pairs={{0,2},{1,3},{2,0},{3,1},{4,6},{5,7},{6,4},{7,5},{8,10},{9,11},{10,... | collective-permute-start | bytes 491528 | tf_op jit(solution)/shard_map/ppermute | solution.py:404
  93.2 3.8 %collective-permute-start.28 = (bf16[80,512]{1,0:T(8,128)(2,1)S(1)}, bf16[80,512]{1,0:T(8,128)(2,1)S(1)}, u32[]{:S(2)}, u32[]{:S(2)}) collective-permute-start(bf16[80,512]{1,0:T(8,128)(2,1)S(1)} %get-tuple-element.85), channel_id=1, source_target_pairs={{0,20},{4,16},{8,28},{12,24},{16,4},{20,0},{24,12},{28,8},{1,21},{... | collective-permute-start | bytes 245768 | tf_op jit(solution)/shard_map/ppermute | solution.py:404
  97.5 3.3 %collective-permute-start.30 = (bf16[80,512]{1,0:T(8,128)(2,1)S(1)}, bf16[80,512]{1,0:T(8,128)(2,1)S(1)}, u32[]{:S(2)}, u32[]{:S(2)}) collective-permute-start(bf16[80,512]{1,0:T(8,128)(2,1)S(1)} %get-tuple-element.88), channel_id=1, source_target_pairs={{0,24},{4,28},{8,16},{12,20},{16,8},{20,12},{24,0},{28,4},{1,25},{... | collective-permute-start | bytes 245768 | tf_op jit(solution)/shard_map/ppermute | solution.py:404
  101.5 4.8 %mixer_close.1 = bf16[1024,384]{1,0:T(8,128)(2,1)} custom-call(s32[2]{0:T(128)S(1)} %pad_add_fusion.ids_ref, f32[1024,128]{1,0:T(8,128)S(1)} %get-tuple-element.51.pre_ref, f32[16,128]{1,0:T(8,128)S(1)} %get-tuple-element.52.dec_ref, bf16[1056,128]{1,0:T(8,128)(2,1)S(1)} %collective-permute-done.3.recv_ref, bf16[1024,384]{1,0:T(8,128)(2,1)S(1)} %get-tuple-element.54.xs_ref, ...), custom_call_target="tpu_custom_call" | custom-call | flops 1500000000 | tf_op jit(solution)/shard_map/mixer_close/pallas_call | solution.py:59
  106.6 1.5 %collective-permute-done.31.refs_4_ = bf16[80,512]{1,0:T(8,128)(2,1)S(1)} collective-permute-done((bf16[80,512]{1,0:T(8,128)(2,1)S(1)}, bf16[80,512]{1,0:T(8,128)(2,1)S(1)}, u32[]{:S(2)}, u32[]{:S(2)}) %collective-permute-start.31) | collective-permute-done | bytes 81952 | tf_op jit(solution)/shard_map/ppermute | solution.py:404
  108.1 1.7 %final_combine.1 = bf16[160,512]{1,0:T(8,128)(2,1)} custom-call(s32[2]{0:T(128)S(1)} %pad_add_fusion.ids_ref, f32[160,8]{1,0:T(8,128)S(1)} %get-tuple-element.58.table_ref, f32[160,512]{1,0:T(8,128)S(1)} %get-tuple-element.77.keep_ref, bf16[160,512]{1,0:T(8,128)(2,1)S(1)} %collective-permute-done.24.refs_0_, ...), custom_call_target="tpu_custom_call" | custom-call | flops 250000000 | tf_op jit(solution)/shard_map/final_combine/pallas_call | solution.py:51
  (51 shorter events, 12.4 us)
Async XLA Ops:
  3.4 12.7 %collective-permute-start.10 = (bf16[80,512]{1,0:T(8,128)(2,1)S(1)}, bf16[80,512]{1,0:T(8,128)(2,1)S(1)}, u32[]{:S(2)}, u32[]{:S(2)}) collective-permute-start(bf16[80,512]{1,0:T(8,128)(2,1)S(1)} %get-tuple-element.63), channel_id=1, source_target_pairs={{0,16},{4,20},{8,24},{12,28},{16,0},{20,4},{24,8},{28,12},{1,17},{... | collective-permute-start | bytes 245768 | tf_op jit(solution)/shard_map/ppermute | solution.py:404
  7.6 19.1 %collective-permute-start = (bf16[16,1280]{1,0:T(8,128)(2,1)S(1)}, bf16[16,1280]{1,0:T(8,128)(2,1)S(1)}, u32[]{:S(2)}, u32[]{:S(2)}) collective-permute-start(bf16[16,1280]{1,0:T(8,128)(2,1)S(1)} %get-tuple-element.46), channel_id=1, source_target_pairs={{0,4},{4,8},{8,12},{12,16},{16,20},{20,24},{24,28},{1,5},{5,9},{9,... | collective-permute-start | bytes 122888 | tf_op jit(solution)/shard_map/ppermute | solution.py:689
  11.0 15.6 %collective-permute-start.11 = (bf16[80,512]{1,0:T(8,128)(2,1)S(1)}, bf16[80,512]{1,0:T(8,128)(2,1)S(1)}, u32[]{:S(2)}, u32[]{:S(2)}) collective-permute-start(bf16[80,512]{1,0:T(8,128)(2,1)S(1)} %get-tuple-element.64), channel_id=1, source_target_pairs={{0,20},{4,16},{8,28},{12,24},{16,4},{20,0},{24,12},{28,8},{1,21},{... | collective-permute-start | bytes 245768 | tf_op jit(solution)/shard_map/ppermute | solution.py:404
  12.3 6.2 %collective-permute-start.13 = (bf16[80,512]{1,0:T(8,128)(2,1)S(1)}, bf16[80,512]{1,0:T(8,128)(2,1)S(1)}, u32[]{:S(2)}, u32[]{:S(2)}) collective-permute-start(bf16[80,512]{1,0:T(8,128)(2,1)S(1)} %get-tuple-element.65), channel_id=1, source_target_pairs={{0,24},{4,28},{8,16},{12,20},{16,8},{20,12},{24,0},{28,4},{1,25},{... | collective-permute-start | bytes 245768 | tf_op jit(solution)/shard_map/ppermute | solution.py:404
  14.4 9.8 %collective-permute-start.14 = (bf16[80,512]{1,0:T(8,128)(2,1)S(1)}, bf16[80,512]{1,0:T(8,128)(2,1)S(1)}, u32[]{:S(2)}, u32[]{:S(2)}) collective-permute-start(bf16[80,512]{1,0:T(8,128)(2,1)S(1)} %get-tuple-element.66), channel_id=1, source_target_pairs={{0,28},{4,24},{8,20},{12,16},{16,12},{20,8},{24,4},{28,0},{1,29},{... | collective-permute-start | bytes 245768 | tf_op jit(solution)/shard_map/ppermute | solution.py:404
  16.1 12.1 %collective-permute-start.4 = (bf16[80,1024]{1,0:T(8,128)(2,1)S(1)}, bf16[80,1024]{1,0:T(8,128)(2,1)S(1)}, u32[]{:S(2)}, u32[]{:S(2)}) collective-permute-start(bf16[80,1024]{1,0:T(8,128)(2,1)S(1)} %get-tuple-element.60), channel_id=1, source_target_pairs={{0,4},{4,0},{8,12},{12,8},{16,20},{20,16},{24,28},{28,24},{1,5},{5... | collective-permute-start | bytes 491528 | tf_op jit(solution)/shard_map/ppermute | solution.py:404
  18.6 10.7 %collective-permute-start.5 = (bf16[80,1024]{1,0:T(8,128)(2,1)S(1)}, bf16[80,1024]{1,0:T(8,128)(2,1)S(1)}, u32[]{:S(2)}, u32[]{:S(2)}) collective-permute-start(bf16[80,1024]{1,0:T(8,128)(2,1)S(1)} %get-tuple-element.61), channel_id=1, source_target_pairs={{0,8},{4,12},{8,0},{12,4},{16,24},{20,28},{24,16},{28,20},{1,9},{5... | collective-permute-start | bytes 491528 | tf_op jit(solution)/shard_map/ppermute | solution.py:404
  24.2 7.5 %collective-permute-start.6 = (bf16[80,1024]{1,0:T(8,128)(2,1)S(1)}, bf16[80,1024]{1,0:T(8,128)(2,1)S(1)}, u32[]{:S(2)}, u32[]{:S(2)}) collective-permute-start(bf16[80,1024]{1,0:T(8,128)(2,1)S(1)} %get-tuple-element.62), channel_id=1, source_target_pairs={{0,12},{4,8},{8,4},{12,0},{16,28},{20,24},{24,20},{28,16},{1,13},{... | collective-permute-start | bytes 491528 | tf_op jit(solution)/shard_map/ppermute | solution.py:404
  26.6 5.2 %collective-permute-start.18 = (bf16[160,512]{1,0:T(8,128)(2,1)S(1)}, bf16[160,512]{1,0:T(8,128)(2,1)S(1)}, u32[]{:S(2)}, u32[]{:S(2)}) collective-permute-start(bf16[160,512]{1,0:T(8,128)(2,1)S(1)} %constant_dynamic-update-slice_fusion.2.refs_9_), channel_id=1, source_target_pairs={{0,1},{1,0},{2,3},{3,2},{4,5},{5,4},{6,7},{7,6},{8,9},{9,8},{10,11... | collective-permute-start | bytes 491528 | tf_op jit(solution)/shard_map/ppermute | solution.py:404
  26.7 7.1 %collective-permute-start.15 = (bf16[160,512]{1,0:T(8,128)(2,1)S(1)}, bf16[160,512]{1,0:T(8,128)(2,1)S(1)}, u32[]{:S(2)}, u32[]{:S(2)}) collective-permute-start(bf16[160,512]{1,0:T(8,128)(2,1)S(1)} %constant_dynamic-update-slice_fusion.2.refs_9_), channel_id=1, source_target_pairs={{0,2},{1,3},{2,0},{3,1},{4,6},{5,7},{6,4},{7,5},{8,10},{9,11},{10,... | collective-permute-start | bytes 491528 | tf_op jit(solution)/shard_map/ppermute | solution.py:404
  28.2 5.6 %collective-permute-start.16 = (bf16[160,512]{1,0:T(8,128)(2,1)S(1)}, bf16[160,512]{1,0:T(8,128)(2,1)S(1)}, u32[]{:S(2)}, u32[]{:S(2)}) collective-permute-start(bf16[160,512]{1,0:T(8,128)(2,1)S(1)} %constant_dynamic-update-slice_fusion.refs_7_), channel_id=1, source_target_pairs={{0,1},{1,0},{2,3},{3,2},{4,5},{5,4},{6,7},{7,6},{8,9},{9,8},{10,11... | collective-permute-start | bytes 491528 | tf_op jit(solution)/shard_map/ppermute | solution.py:404
  29.2 7.6 %collective-permute-start.12 = (bf16[160,512]{1,0:T(8,128)(2,1)S(1)}, bf16[160,512]{1,0:T(8,128)(2,1)S(1)}, u32[]{:S(2)}, u32[]{:S(2)}) collective-permute-start(bf16[160,512]{1,0:T(8,128)(2,1)S(1)} %constant_dynamic-update-slice_fusion.refs_7_), channel_id=1, source_target_pairs={{0,2},{1,3},{2,0},{3,1},{4,6},{5,7},{6,4},{7,5},{8,10},{9,11},{10,... | collective-permute-start | bytes 491528 | tf_op jit(solution)/shard_map/ppermute | solution.py:404
  31.7 11.7 %collective-permute-start.7 = (bf16[80,1024]{1,0:T(8,128)(2,1)S(1)}, bf16[80,1024]{1,0:T(8,128)(2,1)S(1)}, u32[]{:S(2)}, u32[]{:S(2)}) collective-permute-start(bf16[80,1024]{1,0:T(8,128)(2,1)S(1)} %collective-permute-done.4.refs_1_), channel_id=1, source_target_pairs={{0,1},{1,0},{2,3},{3,2},{4,5},{5,4},{6,7},{7,6},{8,9},{9,8},{10,11... | collective-permute-start | bytes 491528 | tf_op jit(solution)/shard_map/ppermute | solution.py:404
  31.7 11.7 %collective-permute-start.8 = (bf16[80,1024]{1,0:T(8,128)(2,1)S(1)}, bf16[80,1024]{1,0:T(8,128)(2,1)S(1)}, u32[]{:S(2)}, u32[]{:S(2)}) collective-permute-start(bf16[80,1024]{1,0:T(8,128)(2,1)S(1)} %collective-permute-done.5.refs_2_), channel_id=1, source_target_pairs={{0,1},{1,0},{2,3},{3,2},{4,5},{5,4},{6,7},{7,6},{8,9},{9,8},{10,11... | collective-permute-start | bytes 491528 | tf_op jit(solution)/shard_map/ppermute | solution.py:404
  33.8 9.6 %collective-permute-start.9 = (bf16[80,1024]{1,0:T(8,128)(2,1)S(1)}, bf16[80,1024]{1,0:T(8,128)(2,1)S(1)}, u32[]{:S(2)}, u32[]{:S(2)}) collective-permute-start(bf16[80,1024]{1,0:T(8,128)(2,1)S(1)} %collective-permute-done.6.refs_3_), channel_id=1, source_target_pairs={{0,1},{1,0},{2,3},{3,2},{4,5},{5,4},{6,7},{7,6},{8,9},{9,8},{10,11... | collective-permute-start | bytes 491528 | tf_op jit(solution)/shard_map/ppermute | solution.py:404
  33.8 9.6 %collective-permute-start.19 = (bf16[160,512]{1,0:T(8,128)(2,1)S(1)}, bf16[160,512]{1,0:T(8,128)(2,1)S(1)}, u32[]{:S(2)}, u32[]{:S(2)}) collective-permute-start(bf16[160,512]{1,0:T(8,128)(2,1)S(1)} %collective-permute-done.15.refs_10_), channel_id=1, source_target_pairs={{0,1},{1,0},{2,3},{3,2},{4,5},{5,4},{6,7},{7,6},{8,9},{9,8},{10,11... | collective-permute-start | bytes 491528 | tf_op jit(solution)/shard_map/ppermute | solution.py:404
  36.8 6.6 %collective-permute-start.17 = (bf16[160,512]{1,0:T(8,128)(2,1)S(1)}, bf16[160,512]{1,0:T(8,128)(2,1)S(1)}, u32[]{:S(2)}, u32[]{:S(2)}) collective-permute-start(bf16[160,512]{1,0:T(8,128)(2,1)S(1)} %collective-permute-done.12.refs_8_), channel_id=1, source_target_pairs={{0,1},{1,0},{2,3},{3,2},{4,5},{5,4},{6,7},{7,6},{8,9},{9,8},{10,11... | collective-permute-start | bytes 491528 | tf_op jit(solution)/shard_map/ppermute | solution.py:404
  53.9 13.2 %collective-permute-start.20 = (bf16[320,1024]{1,0:T(8,128)(2,1)S(1)}, bf16[320,1024]{1,0:T(8,128)(2,1)S(1)}, u32[]{:S(2)}, u32[]{:S(2)}) collective-permute-start(bf16[320,1024]{1,0:T(8,128)(2,1)S(1)} %get-tuple-element.72), channel_id=1, source_target_pairs={{0,1},{1,0},{2,3},{3,2},{4,5},{5,4},{6,7},{7,6},{8,9},{9,8},{10,11... | collective-permute-start | bytes 1966088 | tf_op jit(solution)/shard_map/ppermute | solution.py:404
  56.9 24.0 %collective-permute-start.25 = (bf16[320,1024]{1,0:T(8,128)(2,1)S(1)}, bf16[320,1024]{1,0:T(8,128)(2,1)S(1)}, u32[]{:S(2)}, u32[]{:S(2)}) collective-permute-start(bf16[320,1024]{1,0:T(8,128)(2,1)S(1)} %get-tuple-element.81), channel_id=1, source_target_pairs={{0,1},{1,0},{2,3},{3,2},{4,5},{5,4},{6,7},{7,6},{8,9},{9,8},{10,11... | collective-permute-start | bytes 1966088 | tf_op jit(solution)/shard_map/ppermute | solution.py:404
  57.0 8.9 %collective-permute-start.1 = (bf16[1056,128]{1,0:T(8,128)(2,1)S(1)}, bf16[1056,128]{1,0:T(8,128)(2,1)S(1)}, u32[]{:S(2)}, u32[]{:S(2)}) collective-permute-start(bf16[1056,128]{1,0:T(8,128)(2,1)S(1)} %get-tuple-element.47.mine_ref), channel_id=1, source_target_pairs={{0,4},{4,0},{8,12},{12,8},{16,20},{20,16},{24,28},{28,24},{1,5},{5... | collective-permute-start | bytes 811016 | tf_op jit(solution)/shard_map/ppermute | solution.py:404
  66.6 8.0 %collective-permute-start.2 = (bf16[1056,128]{1,0:T(8,128)(2,1)S(1)}, bf16[1056,128]{1,0:T(8,128)(2,1)S(1)}, u32[]{:S(2)}, u32[]{:S(2)}) collective-permute-start(bf16[1056,128]{1,0:T(8,128)(2,1)S(1)} %get-tuple-element.48.mine_ref), channel_id=1, source_target_pairs={{0,8},{4,12},{8,0},{12,4},{16,24},{20,28},{24,16},{28,20},{1,9},{5... | collective-permute-start | bytes 811016 | tf_op jit(solution)/shard_map/ppermute | solution.py:404
  67.8 15.4 %collective-permute-start.21 = (bf16[80,1024]{1,0:T(8,128)(2,1)S(1)}, bf16[80,1024]{1,0:T(8,128)(2,1)S(1)}, u32[]{:S(2)}, u32[]{:S(2)}) collective-permute-start(bf16[80,1024]{1,0:T(8,128)(2,1)S(1)} %get-tuple-element.74), channel_id=1, source_target_pairs={{0,4},{4,0},{8,12},{12,8},{16,20},{20,16},{24,28},{28,24},{1,5},{5... | collective-permute-start | bytes 491528 | tf_op jit(solution)/shard_map/ppermute | solution.py:404
  75.4 25.5 %collective-permute-start.3 = (bf16[1056,128]{1,0:T(8,128)(2,1)S(1)}, bf16[1056,128]{1,0:T(8,128)(2,1)S(1)}, u32[]{:S(2)}, u32[]{:S(2)}) collective-permute-start(bf16[1056,128]{1,0:T(8,128)(2,1)S(1)} %get-tuple-element.53), channel_id=1, source_target_pairs={{0,16},{4,20},{8,24},{12,28},{1,17},{5,21},{9,25},{13,29},{2,18},{... | collective-permute-start | bytes 811016 | tf_op jit(solution)/shard_map/ppermute | solution.py:722
  78.3 9.7 %collective-permute-start.22 = (bf16[80,1024]{1,0:T(8,128)(2,1)S(1)}, bf16[80,1024]{1,0:T(8,128)(2,1)S(1)}, u32[]{:S(2)}, u32[]{:S(2)}) collective-permute-start(bf16[80,1024]{1,0:T(8,128)(2,1)S(1)} %get-tuple-element.75), channel_id=1, source_target_pairs={{0,8},{4,12},{8,0},{12,4},{16,24},{20,28},{24,16},{28,20},{1,9},{5... | collective-permute-start | bytes 491528 | tf_op jit(solution)/shard_map/ppermute | solution.py:404
  79.8 10.0 %collective-permute-start.23 = (bf16[80,1024]{1,0:T(8,128)(2,1)S(1)}, bf16[80,1024]{1,0:T(8,128)(2,1)S(1)}, u32[]{:S(2)}, u32[]{:S(2)}) collective-permute-start(bf16[80,1024]{1,0:T(8,128)(2,1)S(1)} %get-tuple-element.76), channel_id=1, source_target_pairs={{0,12},{4,8},{8,4},{12,0},{16,28},{20,24},{24,20},{28,16},{1,13},{... | collective-permute-start | bytes 491528 | tf_op jit(solution)/shard_map/ppermute | solution.py:404
  81.7 10.8 %collective-permute-start.26 = (bf16[160,512]{1,0:T(8,128)(2,1)S(1)}, bf16[160,512]{1,0:T(8,128)(2,1)S(1)}, u32[]{:S(2)}, u32[]{:S(2)}) collective-permute-start(bf16[160,512]{1,0:T(8,128)(2,1)S(1)} %get-tuple-element.83), channel_id=1, source_target_pairs={{0,2},{1,3},{2,0},{3,1},{4,6},{5,7},{6,4},{7,5},{8,10},{9,11},{10,... | collective-permute-start | bytes 491528 | tf_op jit(solution)/shard_map/ppermute | solution.py:404
  83.3 13.7 %collective-permute-start.29 = (bf16[160,512]{1,0:T(8,128)(2,1)S(1)}, bf16[160,512]{1,0:T(8,128)(2,1)S(1)}, u32[]{:S(2)}, u32[]{:S(2)}) collective-permute-start(bf16[160,512]{1,0:T(8,128)(2,1)S(1)} %get-tuple-element.87), channel_id=1, source_target_pairs={{0,2},{1,3},{2,0},{3,1},{4,6},{5,7},{6,4},{7,5},{8,10},{9,11},{10,... | collective-permute-start | bytes 491528 | tf_op jit(solution)/shard_map/ppermute | solution.py:404
  90.9 17.2 %collective-permute-start.24 = (bf16[160,512]{1,0:T(8,128)(2,1)S(1)}, bf16[160,512]{1,0:T(8,128)(2,1)S(1)}, u32[]{:S(2)}, u32[]{:S(2)}) collective-permute-start(bf16[160,512]{1,0:T(8,128)(2,1)S(1)} %get-tuple-element.78), channel_id=1, source_target_pairs={{0,2},{1,3},{2,0},{3,1},{4,6},{5,7},{6,4},{7,5},{8,10},{9,11},{10,... | collective-permute-start | bytes 491528 | tf_op jit(solution)/shard_map/ppermute | solution.py:404
  93.1 13.2 %collective-permute-start.27 = (bf16[80,512]{1,0:T(8,128)(2,1)S(1)}, bf16[80,512]{1,0:T(8,128)(2,1)S(1)}, u32[]{:S(2)}, u32[]{:S(2)}) collective-permute-start(bf16[80,512]{1,0:T(8,128)(2,1)S(1)} %get-tuple-element.84), channel_id=1, source_target_pairs={{0,16},{4,20},{8,24},{12,28},{16,0},{20,4},{24,8},{28,12},{1,17},{... | collective-permute-start | bytes 245768 | tf_op jit(solution)/shard_map/ppermute | solution.py:404
  93.2 13.4 %collective-permute-start.28 = (bf16[80,512]{1,0:T(8,128)(2,1)S(1)}, bf16[80,512]{1,0:T(8,128)(2,1)S(1)}, u32[]{:S(2)}, u32[]{:S(2)}) collective-permute-start(bf16[80,512]{1,0:T(8,128)(2,1)S(1)} %get-tuple-element.85), channel_id=1, source_target_pairs={{0,20},{4,16},{8,28},{12,24},{16,4},{20,0},{24,12},{28,8},{1,21},{... | collective-permute-start | bytes 245768 | tf_op jit(solution)/shard_map/ppermute | solution.py:404
  97.5 9.0 %collective-permute-start.30 = (bf16[80,512]{1,0:T(8,128)(2,1)S(1)}, bf16[80,512]{1,0:T(8,128)(2,1)S(1)}, u32[]{:S(2)}, u32[]{:S(2)}) collective-permute-start(bf16[80,512]{1,0:T(8,128)(2,1)S(1)} %get-tuple-element.88), channel_id=1, source_target_pairs={{0,24},{4,28},{8,16},{12,20},{16,8},{20,12},{24,0},{28,4},{1,25},{... | collective-permute-start | bytes 245768 | tf_op jit(solution)/shard_map/ppermute | solution.py:404
  100.9 7.2 %collective-permute-start.31 = (bf16[80,512]{1,0:T(8,128)(2,1)S(1)}, bf16[80,512]{1,0:T(8,128)(2,1)S(1)}, u32[]{:S(2)}, u32[]{:S(2)}) collective-permute-start(bf16[80,512]{1,0:T(8,128)(2,1)S(1)} %get-tuple-element.89), channel_id=1, source_target_pairs={{0,28},{4,24},{8,20},{12,16},{16,12},{20,8},{24,4},{28,0},{1,29},{... | collective-permute-start | bytes 245768 | tf_op jit(solution)/shard_map/ppermute | solution.py:404
where the time goes:
time: 110 us
  starting transfers between devices  46.3 us (42%)
  Pallas kernels  33.8 us (31%)
  waiting for transfers between devices  28.7 us (26%)
    ppermute x30, starting transfers between devices, swap(): return lax.ppermute(value, axis, [(i, i ^ step) for i in range(count)])  40 us
    ppermute x30, waiting for transfers between devices, swap(): return lax.ppermute(value, axis, [(i, i ^ step) for i in range(count)])  28.7 us
    pallas_call x12, Pallas kernels, launch(): pl.pallas_call(body, in_specs=[pl.BlockSpec(memory_space=pltpu.SMEM)] + (...  22.4 us
    pallas_call x2, Pallas kernels, launch(): pl.pallas_call(body, grid_spec=pltpu.PrefetchScalarGridSpec(num_scalar_pr...  11.4 us
    ppermute x1, starting transfers between devices, block(): rims = lax.ppermute(own_rims, 'ep', [(i, i + 1) for i in range(ep - 1)])  3.38 us
    ppermute x1, starting transfers between devices, block(): last = lax.ppermute(message, 'ep', [(i, i + top) for i in range(ep - top)])  2.91 us
  transfers between devices with their start and end apart: 32, of which 11 were waited for; matrix products, arithmetic and copies ran while one was open for 0% of the time, Pallas kernels for 17%

commit v1 on v0

--- a/solution.py
+++ b/solution.py
@@ -19,10 +19,6 @@
 
 def sds(shape, dtype):
     return jax.ShapeDtypeStruct(shape, dtype)
-
-
-def whole(shape):
-    return pl.BlockSpec(shape, lambda *a: (0,) * len(shape))
 
 
 def dot(a, b):
@@ -111,29 +107,31 @@
     return first * capacity + rank_a, second * capacity + rank_b
 
 
-def prep(ids, moe_rows, moe_gain, routes_t, logit_t, x_in, b_in, c_in, sizes):
+def prep(ids, moe_rows, moe_gain, routes_t, logit_t, mixer_args, sizes):
+    x_in, b_in, _ = mixer_args[:3]
     tokens, features = moe_rows.shape
     experts, cap, width, y_count = sizes
     half = experts // 2
     value_rows, length = x_in.shape
     group_rows = b_in.shape[0] // GROUPS
 
-    def body(ids_ref, rows_hbm, gain_hbm, routes_hbm, logit_hbm, x_hbm, b_hbm, c_hbm, *refs):
-        outs, scratch = refs[:-9], refs[-9:]
+    def body(ids_ref, rows_hbm, gain_hbm, routes_hbm, logit_hbm, *refs):
+        count = len(mixer_args)
+        mixer_hbm, outs, scratch = refs[:count], refs[count:-6], refs[-6:]
         normed_ref, sems = scratch[0], scratch[-1]
-        rows_ref, gain_ref, routes_ref, logit_ref, x_ref, b_ref, c_ref = scratch[1:-1]
+        rows_ref, gain_ref, routes_ref, logit_ref = scratch[1:-1]
         self_ref, near, far = outs[0], outs[1:half], outs[half : 2 * half]
-        table_ref, rim_ref = outs[-2:]
+        table_ref, rim_ref = outs[2 * half : 2 * half + 2]
+        mixer_vmem = outs[2 * half + 2 :]
+        x_ref, b_ref, c_ref = mixer_vmem[:3]
         place, y, core = ids_of(ids_ref)
-        tail = (slice(None), slice(length - 128, length))
+        tail = slice(length - 128, length)
         moves = (
             (rows_hbm, rows_ref),
             (gain_hbm, gain_ref),
             (routes_hbm, routes_ref),
             (logit_hbm, logit_ref),
-            (x_hbm.at[tail], x_ref),
-            (b_hbm.at[tail], b_ref),
-            (c_hbm.at[tail], c_ref),
+            *zip(mixer_hbm, mixer_vmem),
         )
         copies = [
             pltpu.make_async_copy(source, target, sems.at[index])
@@ -141,7 +139,7 @@
         ]
         for copy in copies:
             copy.start()
-        for copy in copies:
+        for copy in copies[:4]:
             copy.wait()
         rows = rows_ref[...].astype(F32)
         scale = lax.rsqrt(jnp.mean(rows * rows, axis=1, keepdims=True) + ROW_EPS)
@@ -168,48 +166,48 @@
         table_ref[...] = jnp.transpose(
             fill_rows([dest_a.astype(F32), dest_b.astype(F32)] + shares)
         )
+        for copy in copies[4:]:
+            copy.wait()
         group = y * (GROUPS * 2) // (2 * y_count)
         start = pl.multiple_of(group * group_rows, group_rows)
-        tail = lax.broadcasted_iota(jnp.int32, (16, 128), 0)
+        line = lax.broadcasted_iota(jnp.int32, (16, 128), 0)
         lane = lax.broadcasted_iota(jnp.int32, (16, 128), 1)
-        take = (lane == tail + 125).astype(F32).astype(BF)
+        take = (lane == line + 125).astype(F32).astype(BF)
         nt = (((1,), (1,)), ((), ()))
 
         def edge(block):
             return lax.dot_general(take, block, nt, preferred_element_type=F32).astype(BF)
 
-        rim_ref[:, :value_rows] = edge(x_ref[...])
-        rim_ref[:, value_rows : value_rows + group_rows] = edge(b_ref[pl.ds(start, group_rows), :])
-        rim_ref[:, value_rows + group_rows :] = edge(c_ref[pl.ds(start, group_rows), :])
+        rim_ref[:, :value_rows] = edge(x_ref[:, tail])
+        rim_ref[:, value_rows : value_rows + group_rows] = edge(b_ref[pl.ds(start, group_rows), tail])
+        rim_ref[:, value_rows + group_rows :] = edge(c_ref[pl.ds(start, group_rows), tail])
 
     outs = [sds((cap, features), BF)]
     outs += [sds((cap, y_count * width), BF)] * (half - 1)
     outs += [sds((cap, width), BF)] * half
     outs += [sds((tokens, 8), F32), sds((16, value_rows + 2 * group_rows), BF)]
+    outs += [sds(a.shape, a.dtype) for a in mixer_args]
     return call(
         body,
         "prep",
         ids,
-        tuple(map(in_hbm, (moe_rows, moe_gain, routes_t, logit_t, x_in, b_in, c_in))),
+        tuple(map(in_hbm, (moe_rows, moe_gain, routes_t, logit_t, *mixer_args))),
         outs,
-        in_specs=[pl.BlockSpec(memory_space=pltpu.HBM)] * 7,
+        in_specs=[pl.BlockSpec(memory_space=pltpu.HBM)] * (4 + len(mixer_args)),
         scratch=[
             pltpu.VMEM((tokens, features), BF),
             pltpu.VMEM(moe_rows.shape, BF),
             pltpu.VMEM(moe_gain.shape, F32),
             pltpu.VMEM(routes_t.shape, jnp.int32),
             pltpu.VMEM(logit_t.shape, F32),
-            pltpu.VMEM((value_rows, 128), BF),
-            pltpu.VMEM((b_in.shape[0], 128), BF),
-            pltpu.VMEM((c_in.shape[0], 128), BF),
-            pltpu.SemaphoreType.DMA((7,)),
+            pltpu.SemaphoreType.DMA((4 + len(mixer_args),)),
         ],
         us=3.0,
         mib=10,
     )
 
 
-def gate_up(ids, self_rows, near, near_other, far, far_other, w_gate, w_up, w_down, sizes):
+def gate_up(ids, self_rows, near, near_other, far, far_other, w_gate, w_up, w_down, z_in, sizes):
     experts, cap, width, y_count = sizes
     features, hidden = w_gate.shape[1:]
     rows = experts * cap
@@ -219,9 +217,13 @@
     pieces = (self_rows, *(value for group in groups for value in group))
 
     def body(ids_ref, *refs):
-        wg_ref, wu_ref, wd_ref, low_ref, high_ref, held_ref, lhs_ref, sem = refs[len(pieces) :]
-        copy = pltpu.make_async_copy(wd_ref, held_ref, sem)
-        copy.start()
+        wg_ref, wu_ref, wd_ref, z_ref, low_ref, high_ref, held_ref, held_z_ref, lhs_ref, sems = refs[len(pieces) :]
+        copies = [
+            pltpu.make_async_copy(wd_ref, held_ref, sems.at[0]),
+            pltpu.make_async_copy(z_ref, held_z_ref, sems.at[1]),
+        ]
+        for copy in copies:
+            copy.start()
         at, held = 1, []
         for group in groups:
             held.append(refs[at : at + len(group)])
@@ -253,17 +255,18 @@
                 gate = dot(lhs, wg_ref[0, :, span])
                 up = dot(lhs, wu_ref[0, :, span])
                 out_ref[:, span] = (silu(gate) * up).astype(BF)
-        copy.wait()
+        for copy in copies:
+            copy.wait()
 
     vmem = pl.BlockSpec(memory_space=pltpu.VMEM)
     return call(
         body,
         "gate_up",
         ids,
-        (*pieces, w_gate, w_up, in_hbm(w_down)),
-        [sds((split, hidden), BF)] * 2 + [sds(w_down.shape, w_down.dtype)],
-        in_specs=[vmem] * (len(pieces) + 2) + [pl.BlockSpec(memory_space=pltpu.HBM)],
-        scratch=[pltpu.VMEM((rows, features), BF), pltpu.SemaphoreType.DMA],
+        (*pieces, w_gate, w_up, in_hbm(w_down), in_hbm(z_in)),
+        [sds((split, hidden), BF)] * 2 + [sds(w_down.shape, BF), sds(z_in.shape, BF)],
+        in_specs=[vmem] * (len(pieces) + 2) + [pl.BlockSpec(memory_space=pltpu.HBM)] * 2,
+        scratch=[pltpu.VMEM((rows, features), BF), pltpu.SemaphoreType.DMA((2,))],
         us=9.0,
         mib=GATE_MIB,
     )
@@ -430,142 +433,163 @@
     )
 
 
-def mixer_open(ids, x_in, dt_raw, rate_row, b_in, c_in, taps_x, taps_b, taps_c, rims, weights, hb, hp, y_count):
+def sent_decay(total, hp):
+    count, width = total.shape
+    if count < hp:
+        total = jnp.concatenate([total, jnp.ones((hp - count, width), F32)], axis=0)
+    high = total.astype(BF)
+    return high, (total - high.astype(F32)).astype(BF)
+
+
+def decay_of(ref, rows, hp):
+    return ref[rows : rows + hp, :].astype(F32) + ref[rows + hp :, :].astype(F32)
+
+
+def span_state(signal, rim, taps, step, cum, b_t, xs_ref, msg_ref, hb, hp):
+    rows, length = signal.shape
+    value = conv_block(signal, rim, taps)
+    last = cum[:, length - 1 : length]
+    scaled = value * head_rows(step, hb, length)
+    xs_ref[...] = scaled.astype(BF)
+    state = dot((scaled * head_rows(jnp.exp(last - cum), hb, length)).astype(BF), b_t)
+    msg_ref[:rows, :] = state.astype(BF)
+    high, low = sent_decay(jnp.broadcast_to(jnp.exp(last), (hb, NSTATE)), hp)
+    msg_ref[rows : rows + hp, :] = high
+    msg_ref[rows + hp :, :] = low
+
+
+def mixer_open_a(ids, x_in, dt_raw, rate_row, b_in, c_in, taps_x, taps_b, taps_c, rims, weight, hb, hp, y_count):
     rows, length = x_in.shape
     heads = dt_raw.shape[0]
-    block_rows = hb * HEAD_DIM
-
-    def body(ids_ref, x_ref, dt_ref, rate_ref, b_ref, c_ref, tx_ref, tb_ref, tc_ref, rim_ref, *refs):
-        from_refs, outs = refs[: len(weights)], refs[len(weights) :]
-        xs_ref, cum_ref, bt_ref, conv_c_ref, msg_ref = outs[:5]
-        into_refs, (step_ref, sems) = outs[5:-2], outs[-2:]
-        copies = [
-            pltpu.make_async_copy(source, target, sems.at[index])
-            for index, (source, target) in enumerate(zip(from_refs, into_refs))
-        ]
+    part = hb * HEAD_DIM
+
+    def body(ids_ref, x_ref, dt_ref, rate_ref, b_ref, c_ref, tx_ref, tb_ref, tc_ref, rim_ref, w_ref, *outs):
+        xs_ref, cum_a_ref, cum_b_ref, step_ref, bt_ref, conv_c_ref, msg_ref, into_ref, sem = outs
+        copy = pltpu.make_async_copy(w_ref, into_ref, sem)
+        copy.start()
         _, y, _ = ids_of(ids_ref)
-        turn = pl.program_id(0)
-
-        @pl.when(turn == 0)
-        def _():
-            for copy in copies:
-                copy.start()
-            group = y * (GROUPS * 2) // (2 * y_count)
-            start = pl.multiple_of(group * NSTATE, NSTATE)
-            span = pl.ds(start, NSTATE)
-            b_conv = conv_block(b_ref[span, :], rim_ref[:, rows : rows + NSTATE], tb_ref[:, span])
-            c_conv = conv_block(c_ref[span, :], rim_ref[:, rows + NSTATE :], tc_ref[:, span])
-            bt_ref[...] = jnp.transpose(b_conv).astype(BF)
-            conv_c_ref[...] = c_conv.astype(BF)
-            raw = dt_ref[...]
-            step = jnp.maximum(raw, 0.0) + jnp.log1p(jnp.exp(-jnp.abs(raw)))
-            eye_r = lax.broadcasted_iota(jnp.int32, (heads, heads), 0)
-            eye_c = lax.broadcasted_iota(jnp.int32, (heads, heads), 1)
-            rate = jnp.sum(jnp.where(eye_r == eye_c, rate_ref[...], 0.0), axis=1, keepdims=True)
-            cum = -step * rate
-            lane = lax.broadcasted_iota(jnp.int32, (heads, length), 1)
-            shift = 1
-            while shift < length:
-                cum = cum + jnp.where(lane >= shift, pltpu.roll(cum, shift, 1), 0.0)
-                shift *= 2
-            step_ref[...] = step
-            cum_ref[...] = cum
-            total = jnp.broadcast_to(jnp.exp(cum[:, length - 1 : length]), (heads, NSTATE))
-            if heads < hp:
-                total = jnp.concatenate([total, jnp.ones((hp - heads, NSTATE), F32)], axis=0)
-            high = total.astype(BF)
-            msg_ref[rows : rows + hp, :] = high
-            msg_ref[rows + hp : rows + 2 * hp, :] = (total - high.astype(F32)).astype(BF)
-
-        value = conv_block(x_ref[...], rim_ref[:, pl.ds(pl.multiple_of(turn * block_rows, block_rows), block_rows)], tx_ref[...])
-        first = turn * hb if heads > hb else 0
-        step = step_ref[pl.ds(first, hb), :]
-        cum = cum_ref[pl.ds(first, hb), :]
-        fade = jnp.exp(cum[:, length - 1 : length] - cum)
-        scaled = value * head_rows(step, hb, length)
-        xs_ref[...] = scaled.astype(BF)
-        state = dot((scaled * head_rows(fade, hb, length)).astype(BF), bt_ref[...])
-        msg_ref[pl.ds(pl.multiple_of(turn * block_rows, block_rows), block_rows), :] = state.astype(BF)
-
-        @pl.when(turn == heads // hb - 1)
-        def _():
-            for copy in copies:
-                copy.wait()
-
+        group = y * (GROUPS * 2) // (2 * y_count)
+        start = pl.multiple_of(group * NSTATE, NSTATE)
+        span = pl.ds(start, NSTATE)
+        b_conv = conv_block(b_ref[span, :], rim_ref[:, rows : rows + NSTATE], tb_ref[:, span])
+        c_conv = conv_block(c_ref[span, :], rim_ref[:, rows + NSTATE :], tc_ref[:, span])
+        b_t = jnp.transpose(b_conv).astype(BF)
+        bt_ref[...] = b_t
+        conv_c_ref[...] = c_conv.astype(BF)
+        raw = dt_ref[...]
+        step = jnp.maximum(raw, 0.0) + jnp.log1p(jnp.exp(-jnp.abs(raw)))
+        eye_r = lax.broadcasted_iota(jnp.int32, (heads, heads), 0)
+        eye_c = lax.broadcasted_iota(jnp.int32, (heads, heads), 1)
+        rate = jnp.sum(jnp.where(eye_r == eye_c, rate_ref[...], 0.0), axis=1, keepdims=True)
+        cum = -step * rate
+        lane = lax.broadcasted_iota(jnp.int32, (heads, length), 1)
+        shift = 1
+        while shift < length:
+            cum = cum + jnp.where(lane >= shift, pltpu.roll(cum, shift, 1), 0.0)
+            shift *= 2
+        step_ref[...] = step[hb:]
+        cum_a_ref[...] = cum[:hb]
+        cum_b_ref[...] = cum[hb:]
+        span_state(x_ref[:part, :], rim_ref[:, :part], tx_ref[:, :part], step[:hb], cum[:hb], b_t, xs_ref, msg_ref, hb, hp)
+        copy.wait()
+
+    vmem = pl.BlockSpec(memory_space=pltpu.VMEM)
     outs = [
-        sds((rows, length), BF),
-        sds((heads, length), F32),
+        sds((part, length), BF),
+        sds((hb, length), F32),
+        sds((hb, length), F32),
+        sds((hb, length), F32),
         sds((length, NSTATE), BF),
         sds((NSTATE, length), BF),
-        sds((rows + 2 * hp, NSTATE), BF),
-    ] + [sds(w.shape, w.dtype) for w in weights]
-    vmem = pl.BlockSpec(memory_space=pltpu.VMEM)
+        sds((part + 2 * hp, NSTATE), BF),
+        sds(weight.shape, weight.dtype),
+    ]
     return call(
         body,
-        "mixer_open",
+        "mixer_open_a",
         ids,
-        (*map(in_hbm, (x_in, dt_raw, rate_row, b_in, c_in, taps_x, taps_b, taps_c)), rims, *map(in_hbm, weights)),
+        (x_in, dt_raw, rate_row, b_in, c_in, taps_x, taps_b, taps_c, rims, in_hbm(weight)),
         outs,
-        grid=(heads // hb,),
-        in_specs=[
-            pl.BlockSpec((block_rows, length), lambda i, s: (i, 0)),
-            whole(dt_raw.shape),
-            whole(rate_row.shape),
-            whole(b_in.shape),
-            whole(c_in.shape),
-            pl.BlockSpec((taps_x.shape[0], block_rows), lambda i, s: (0, i)),
-            whole(taps_b.shape),
-            whole(taps_c.shape),
-            vmem,
-        ]
-        + [pl.BlockSpec(memory_space=pltpu.HBM)] * len(weights),
-        out_specs=[pl.BlockSpec((block_rows, length), lambda i, s: (i, 0))]
-        + [whole(o.shape) for o in outs[1:5]]
-        + [vmem] * len(weights),
-        scratch=[pltpu.VMEM((heads, length), F32), pltpu.SemaphoreType.DMA((len(weights),))],
-        us=7.0,
+        in_specs=[vmem] * 9 + [pl.BlockSpec(memory_space=pltpu.HBM)],
+        out_specs=[vmem] * len(outs),
+        scratch=[pltpu.SemaphoreType.DMA],
+        us=4.0,
         mib=OPEN_MIB,
     )
 
 
-def per_row(table, heads):
-    width = table.shape[1]
-    return jnp.broadcast_to(table[:heads][:, None, :], (heads, HEAD_DIM, width)).reshape(
-        heads * HEAD_DIM, width
-    )
-
-
-def state_round(ids, mine, received, carried, level, heads, hp):
-    rows = heads * HEAD_DIM
+def mixer_open_b(ids, x_in, taps_x, rims, step, cum, b_t, message, weight, hb, hp):
+    rows, length = x_in.shape
+    part = hb * HEAD_DIM
+
+    def body(ids_ref, x_ref, tx_ref, rim_ref, step_ref, cum_ref, bt_ref, other_ref, w_ref, *outs):
+        xs_ref, send_ref, mine_ref, into_ref, msg_ref, sem = outs
+        copy = pltpu.make_async_copy(w_ref, into_ref, sem)
+        copy.start()
+        span_state(
+            x_ref[part:, :], rim_ref[:, part:rows], tx_ref[:, part:], step_ref[...], cum_ref[...], bt_ref[...], xs_ref, msg_ref, hb, hp
+        )
+        odd = ids_ref[0] % 2 == 1
+        a, b = other_ref[...].astype(F32), msg_ref[...].astype(F32)
+        send_ref[...] = jnp.where(odd, a, b).astype(BF)
+        mine_ref[...] = jnp.where(odd, b, a).astype(BF)
+        copy.wait()
+
+    vmem = pl.BlockSpec(memory_space=pltpu.VMEM)
+    outs = [sds((part, length), BF), sds(message.shape, BF), sds(message.shape, BF), sds(weight.shape, weight.dtype)]
+    return call(
+        body,
+        "mixer_open_b",
+        ids,
+        (x_in, taps_x, rims, step, cum, b_t, message, in_hbm(weight)),
+        outs,
+        in_specs=[vmem] * 7 + [pl.BlockSpec(memory_space=pltpu.HBM)],
+        out_specs=[vmem] * len(outs),
+        scratch=[pltpu.VMEM(message.shape, BF), pltpu.SemaphoreType.DMA],
+        us=3.0,
+        mib=OPEN_MIB,
+    )
+
+
+def state_pair(ids, mine, received, hb, hp):
+    rows = hb * HEAD_DIM
+
+    def body(ids_ref, mine_ref, recv_ref, msg_ref):
+        odd = ids_ref[0] % 2 == 1
+        t_mine, t_recv = mine_ref[:rows, :].astype(F32), recv_ref[:rows, :].astype(F32)
+        d_mine, d_recv = decay_of(mine_ref, rows, hp), decay_of(recv_ref, rows, hp)
+        late, early = jnp.where(odd, t_mine, t_recv), jnp.where(odd, t_recv, t_mine)
+        d_late = jnp.where(odd, d_mine, d_recv)
+        msg_ref[:rows, :] = (late + head_rows(d_late, hb, NSTATE) * early).astype(BF)
+        high, low = sent_decay(d_mine * d_recv, hp)
+        msg_ref[rows : rows + hp, :] = high
+        msg_ref[rows + hp :, :] = low
+
+    return call(body, "state_pair", ids, (mine, received), [sds(mine.shape, BF)])[0]
+
+
+def state_round(ids, mine, received, carried, level, hb, hp):
+    rows = hb * HEAD_DIM
     opening = carried is None
     outs = [sds(mine.shape, BF), sds((rows, NSTATE), F32), sds((hp, NSTATE), F32)]
 
     def body(ids_ref, mine_ref, recv_ref, *refs):
         msg_ref, pre_ref, dec_ref = refs[-3:]
         upper = (ids_ref[0] >> level) % 2 == 1
-        t_mine = mine_ref[:rows, :].astype(F32)
-        t_recv = recv_ref[:rows, :].astype(F32)
-
-        def decay(ref):
-            return ref[rows : rows + hp, :].astype(F32) + ref[rows + hp :, :].astype(F32)
-
-        d_mine, d_recv = decay(mine_ref), decay(recv_ref)
-        one = jnp.ones_like(d_mine)
+        t_mine, t_recv = mine_ref[:rows, :].astype(F32), recv_ref[:rows, :].astype(F32)
+        d_mine, d_recv = decay_of(mine_ref, rows, hp), decay_of(recv_ref, rows, hp)
+        late, early = jnp.where(upper, t_mine, t_recv), jnp.where(upper, t_recv, t_mine)
         d_late = jnp.where(upper, d_mine, d_recv)
-        late = jnp.where(upper, t_mine, t_recv)
-        early = jnp.where(upper, t_recv, t_mine)
-        total = late + per_row(d_late, heads) * early
-        msg_ref[:rows, :] = total.astype(BF)
-        both = d_mine * d_recv
-        high = both.astype(BF)
+        msg_ref[:rows, :] = (late + head_rows(d_late, hb, NSTATE) * early).astype(BF)
+        high, low = sent_decay(d_mine * d_recv, hp)
         msg_ref[rows : rows + hp, :] = high
-        msg_ref[rows + hp :, :] = (both - high.astype(F32)).astype(BF)
+        msg_ref[rows + hp :, :] = low
         if opening:
             pre_ref[...] = jnp.where(upper, t_recv, jnp.zeros_like(t_recv))
-            dec_ref[...] = jnp.where(upper, d_recv, one)
+            dec_ref[...] = jnp.where(upper, d_recv, jnp.ones_like(d_recv))
         else:
             old_pre, old_dec = refs[0], refs[1]
-            grown = old_pre[...] + per_row(old_dec[...], heads) * t_recv
+            grown = old_pre[...] + head_rows(old_dec[...], hb, NSTATE) * t_recv
             pre_ref[...] = jnp.where(upper, grown, old_pre[...])
             dec_ref[...] = jnp.where(upper, old_dec[...] * d_recv, old_dec[...])
 
@@ -573,13 +597,28 @@
     return call(body, f"state_round_{level}", ids, ins, outs)
 
 
-def mixer_close(ids, carried, received, xs, cum, b_t, c_conv, z_in, gain_row, hb):
-    rows, length = xs.shape
-    heads = cum.shape[0]
-    block_rows = hb * HEAD_DIM
+def state_finish(ids, mine, pair, carried, last, hb, hp):
+    rows = hb * HEAD_DIM
+
+    def body(ids_ref, mine_ref, pair_ref, pre_ref, dec_ref, last_ref, send_ref, keep_ref):
+        odd = ids_ref[0] % 2 == 1
+        before = pre_ref[...] + head_rows(dec_ref[...], hb, NSTATE) * last_ref[:rows, :].astype(F32)
+        t_even = jnp.where(odd, pair_ref[:rows, :].astype(F32), mine_ref[:rows, :].astype(F32))
+        d_even = jnp.where(odd, decay_of(pair_ref, rows, hp), decay_of(mine_ref, rows, hp))
+        after = head_rows(d_even, hb, NSTATE) * before + t_even
+        send_ref[...] = jnp.where(odd, before, after).astype(BF)
+        keep_ref[...] = jnp.where(odd, after, before).astype(BF)
+
+    outs = [sds((rows, NSTATE), BF)] * 2
+    return call(body, "state_finish", ids, (mine, pair, *carried, last), outs)
+
+
+def mixer_close(ids, keep, received, xs_parts, cum_parts, b_t, c_conv, z_in, gain_row, hb):
+    rows, length = z_in.shape
+    part = hb * HEAD_DIM
     blocks = length // BLOCK
 
-    def body(ids_ref, pre_ref, dec_ref, recv_ref, xs_ref, cum_ref, bt_ref, c_ref, z_ref, gain_ref, out_ref, gram_ref, y_ref):
+    def body(ids_ref, keep_ref, recv_ref, xa_ref, xb_ref, ca_ref, cb_ref, bt_ref, c_ref, z_ref, gain_ref, out_ref, gram_ref, y_ref, xs_ref):
         turn = pl.program_id(0)
 
         @pl.when(turn == 0)
@@ -590,12 +629,15 @@
                 span = slice(j * BLOCK, (j + 1) * BLOCK)
                 gram = dot(bt_ref[span, :], c_ref[:, span])
                 gram_ref[j] = jnp.where(row <= col, gram, 0.0)
-
-        first = turn * hb if heads > hb else 0
-        decay = dec_ref[pl.ds(first, hb), :]
-        own = pl.ds(pl.multiple_of(turn * block_rows, block_rows), block_rows)
-        state = pre_ref[own, :] + head_rows(decay, hb, NSTATE) * recv_ref[own, :].astype(F32)
-        cum = cum_ref[...]
+            xs_ref[...] = xa_ref[...]
+
+        @pl.when(turn == 1)
+        def _():
+            xs_ref[...] = xb_ref[...]
+
+        own = turn == ids_ref[0] % 2
+        state = jnp.where(own, keep_ref[...].astype(F32), recv_ref[...].astype(F32))
+        cum = jnp.where(turn == 0, ca_ref[...], cb_ref[...])
         down_cum = jnp.transpose(fill_rows([cum[i : i + 1, :] for i in range(hb)]))
         before = jnp.zeros((hb, 1), F32)
         for j in range(blocks):
@@ -616,36 +658,30 @@
                 kept = head_rows(jnp.broadcast_to(jnp.exp(after - before), (hb, NSTATE)), hb, NSTATE)
                 state = kept * state + fresh
             before = after
-        gain = tall([gain_ref[...]])
+        gain = tall([gain_ref[:, pl.ds(pl.multiple_of(turn * part, part), part)]])
         for i in range(hb):
             lines = slice(i * HEAD_DIM, (i + 1) * HEAD_DIM)
-            gated = y_ref[lines, :] * silu(z_ref[lines, :].astype(F32))
+            z_lines = pl.ds(pl.multiple_of(turn * part + i * HEAD_DIM, HEAD_DIM), HEAD_DIM)
+            gated = y_ref[lines, :] * silu(z_ref[z_lines, :].astype(F32))
             scale = lax.rsqrt(jnp.mean(gated * gated, axis=0, keepdims=True) + HEAD_EPS)
             out_ref[lines, :] = (gated * scale * gain[lines, 0:1]).astype(BF)
 
-    pre, dec = carried
-    tile = pl.BlockSpec((block_rows, length), lambda i, s: (i, 0))
+    tile = pl.BlockSpec((part, length), lambda i, s: (i, 0))
     vmem = pl.BlockSpec(memory_space=pltpu.VMEM)
     return call(
         body,
         "mixer_close",
         ids,
-        (pre, dec, received, xs, cum, b_t, c_conv, in_hbm(z_in), in_hbm(gain_row)),
+        (keep, received, *xs_parts, *cum_parts, b_t, c_conv, z_in, gain_row),
         [sds((rows, length), BF)],
-        grid=(heads // hb,),
-        in_specs=[
-            vmem,
-            vmem,
-            vmem,
-            tile,
-            pl.BlockSpec((hb, length), lambda i, s: (i, 0)),
-            whole(b_t.shape),
-            whole(c_conv.shape),
-            tile,
-            pl.BlockSpec((1, block_rows), lambda i, s: (0, i)),
+        grid=(2,),
+        in_specs=[vmem] * 10,
+        out_specs=[tile],
+        scratch=[
+            pltpu.VMEM((blocks, BLOCK, BLOCK), F32),
+            pltpu.VMEM((part, length), F32),
+            pltpu.VMEM((part, length), BF),
         ],
-        out_specs=[tile],
-        scratch=[pltpu.VMEM((blocks, BLOCK, BLOCK), F32), pltpu.VMEM((block_rows, length), F32)],
         us=6.0,
         mib=12,
     )[0]
@@ -673,7 +709,8 @@
     ep, tp = lax.axis_size("ep"), lax.axis_size("tp")
     y_count = tp // 2
     heads = dt_raw.shape[0]
-    hb, hp = min(8, heads), -(-heads // 16) * 16
+    hb = heads // 2
+    hp = -(-hb // 16) * 16
     tokens, features = moe_rows.shape
     experts = ep * w_gate.shape[0]
     capacity = 2 * tokens * routes.shape[1] // experts
@@ -683,9 +720,21 @@
     ids = jnp.stack([lax.axis_index("ep"), lax.axis_index("tp")]).astype(jnp.int32)
     routes_t, logit_t = routes.T, route_logit.T
 
-    outs = prep(ids, moe_rows, moe_gain.reshape(1, -1), routes_t, logit_t, x_in, b_in, c_in, sizes)
+    mixer_args = (
+        x_in,
+        b_in,
+        c_in,
+        dt_raw,
+        decay_rate.reshape(1, -1),
+        conv_x.T,
+        conv_b.T,
+        conv_c.T,
+        head_gain.reshape(1, -1),
+    )
+    outs = prep(ids, moe_rows, moe_gain.reshape(1, -1), routes_t, logit_t, mixer_args, sizes)
     self_rows, near, far = outs[0], outs[1:half], outs[half : 2 * half]
-    table, own_rims = outs[-2:]
+    table, own_rims = outs[2 * half : 2 * half + 2]
+    x_in, b_in, c_in, dt_raw, rate_row, taps_x, taps_b, taps_c, gain_row = outs[2 * half + 2 :]
     rims = lax.ppermute(own_rims, "ep", [(i, i + 1) for i in range(ep - 1)])
     far = [swap(value, "ep", half + index) for index, value in enumerate(far)]
     near = [swap(value, "ep", 1 + index) for index, value in enumerate(near)]
@@ -697,32 +746,39 @@
     near_other = [swap(value, "tp", 1) for value in near]
     far_other = [[swap(value, "tp", 1) for value in group] for group in far_sets]
 
-    xs, cum, b_t, c_conv, message, w_gate, w_up = mixer_open(
+    xs_a, cum_a, cum_b, step_b, b_t, c_conv, message, w_gate = mixer_open_a(
         ids,
         x_in,
         dt_raw,
-        decay_rate.reshape(1, -1),
+        rate_row,
         b_in,
         c_in,
-        conv_x.T,
-        conv_b.T,
-        conv_c.T,
+        taps_x,
+        taps_b,
+        taps_c,
         rims,
-        (w_gate, w_up),
+        w_gate,
         hb,
         hp,
         y_count,
     )
-    carried, level = None, 0
+    xs_b, send, mine, w_up = mixer_open_b(
+        ids, x_in, taps_x, rims, step_b, cum_b, b_t, message, w_up, hb, hp
+    )
+    pair = swap(send, "ep", 1)
+    message = state_pair(ids, mine, pair, hb, hp)
+    carried, level = None, 1
     while (2 << level) < ep:
         received = swap(message, "ep", 1 << level)
-        message, *carried = state_round(ids, message, received, carried, level, heads, hp)
+        message, *carried = state_round(ids, message, received, carried, level, hb, hp)
         level += 1
     top = 1 << level
     last = lax.ppermute(message, "ep", [(i, i + top) for i in range(ep - top)])
-
-    hid_near, hid_far, w_down = gate_up(
-        ids, self_rows, near, near_other, far_sets, far_other, w_gate, w_up, w_down, sizes
+    send, keep = state_finish(ids, mine, pair, carried, last, hb, hp)
+    back = swap(send, "ep", 1)
+
+    hid_near, hid_far, w_down, z_in = gate_up(
+        ids, self_rows, near, near_other, far_sets, far_other, w_gate, w_up, w_down, z_in, sizes
     )
     send_far, keep_far = down(ids, hid_far, w_down, sizes, "down_far")
     recv_far = swap(send_far, "tp", 1)
@@ -747,7 +803,16 @@
     moe_t = final_combine(ids, far_back, near_keep, near_received, table, sizes)
 
     mixed = mixer_close(
-        ids, carried, last, xs, cum, b_t, c_conv, z_in, head_gain.reshape(1, -1), hb
+        ids,
+        keep,
+        back,
+        (xs_a, xs_b),
+        (cum_a, cum_b),
+        b_t,
+        c_conv,
+        z_in,
+        gain_row,
+        hb,
     )
     return (mixed, moe_t.T)
 

time: 110 us -> 112 us (1.018)
  waiting for transfers between devices: 28.7 us -> 36.9 us
  starting transfers between devices: 46.3 us -> 40.5 us
    ppermute x30 -> x31, waiting for transfers between devices: 28.7 us -> 36.9 us  [swap(): return lax.ppermute(value, axis, [(i, i ^ step) for i in range(count)])]
    pallas_call x2 -> x1, Pallas kernels: 11.4 us -> 3.9 us  [launch(): pl.pallas_call(body, grid_spec=pltpu.PrefetchScalarGridSpec(num_scalar_pr...]
    pallas_call x12 -> x15, Pallas kernels: 22.4 us -> 29.8 us  [launch(): pl.pallas_call(body, in_specs=[pl.BlockSpec(memory_space=pltpu.SMEM)] + (...]
    ppermute x30 -> x31, starting transfers between devices: 40 us -> 33.6 us  [swap(): return lax.ppermute(value, axis, [(i, i ^ step) for i in range(count)])]
  transfers between devices with their start and end apart: 32 -> 33, of which waited for: 11 -> 10; matrix products, arithmetic and copies ran while one was open for 0% -> 0% of each run, Pallas kernels for 17% -> 17%
where the time goes in v1:
time: 112 us
  starting transfers between devices  40.5 us (36%)
  waiting for transfers between devices  36.9 us (33%)
  Pallas kernels  33.7 us (30%)
    ppermute x31, waiting for transfers between devices, swap(): return lax.ppermute(value, axis, [(i, i ^ step) for i in range(count)])  36.9 us
    ppermute x31, starting transfers between devices, swap(): return lax.ppermute(value, axis, [(i, i ^ step) for i in range(count)])  33.6 us
    pallas_call x15, Pallas kernels, launch(): pl.pallas_call(body, in_specs=[pl.BlockSpec(memory_space=pltpu.SMEM)] + (...  29.8 us
    pallas_call x1, Pallas kernels, launch(): pl.pallas_call(body, grid_spec=pltpu.PrefetchScalarGridSpec(num_scalar_pr...  3.9 us
    ppermute x1, starting transfers between devices, block(): last = lax.ppermute(message, 'ep', [(i, i + top) for i in range(ep - top)])  3.53 us
    ppermute x1, starting transfers between devices, block(): rims = lax.ppermute(own_rims, 'ep', [(i, i + 1) for i in range(ep - 1)])  3.39 us
  transfers between devices with their start and end apart: 33, of which 10 were waited for; matrix products, arithmetic and copies ran while one was open for 0% of the time, Pallas kernels for 17%

profile of v1, /device:TPU:0, one launch (start us, length us, event | category | flops | bytes accessed | tf_op | source)
XLA Modules:
  0.0 112.1 jit_solution(13122766936276883166)
XLA Ops:
  0.7 2.8 %prep.1 = (bf16[80,2048]{1,0:T(8,128)(2,1)S(1)}, bf16[80,1024]{1,0:T(8,128)(2,1)S(1)}, bf16[80,1024]{1,0:T(8,128)(2,1)S(1)}, bf16[80,1024]{1,0:T(8,128)(2,1)S(1)...) custom-call(s32[2]{0:T(128)S(1)} %pad_add_fusion.ids_ref, ...), custom_call_target="tpu_custom_call" | custom-call | flops 750000000 | tf_op jit(solution)/shard_map/prep/pallas_call | solution.py:47
  3.6 4.1 %collective-permute-start.11 = (bf16[80,512]{1,0:T(8,128)(2,1)S(1)}, bf16[80,512]{1,0:T(8,128)(2,1)S(1)}, u32[]{:S(2)}, u32[]{:S(2)}) collective-permute-start(bf16[80,512]{1,0:T(8,128)(2,1)S(1)} %get-tuple-element.88), channel_id=1, source_target_pairs={{0,16},{4,20},{8,24},{12,28},{16,0},{20,4},{24,8},{28,12},{1,17},{... | collective-permute-start | bytes 245768 | tf_op jit(solution)/shard_map/ppermute | solution.py:407
  7.7 3.4 %collective-permute-start = (bf16[16,1280]{1,0:T(8,128)(2,1)S(1)}, bf16[16,1280]{1,0:T(8,128)(2,1)S(1)}, u32[]{:S(2)}, u32[]{:S(2)}) collective-permute-start(bf16[16,1280]{1,0:T(8,128)(2,1)S(1)} %get-tuple-element.62), channel_id=1, source_target_pairs={{0,4},{4,8},{8,12},{12,16},{16,20},{20,24},{24,28},{1,5},{5,9},{9,... | collective-permute-start | bytes 122888 | tf_op jit(solution)/shard_map/ppermute | solution.py:738
  11.1 1.6 %collective-permute-start.5 = (bf16[80,1024]{1,0:T(8,128)(2,1)S(1)}, bf16[80,1024]{1,0:T(8,128)(2,1)S(1)}, u32[]{:S(2)}, u32[]{:S(2)}) collective-permute-start(bf16[80,1024]{1,0:T(8,128)(2,1)S(1)} %get-tuple-element.85), channel_id=1, source_target_pairs={{0,4},{4,0},{8,12},{12,8},{16,20},{20,16},{24,28},{28,24},{1,5},{5... | collective-permute-start | bytes 491528 | tf_op jit(solution)/shard_map/ppermute | solution.py:407
  12.8 1.8 %collective-permute-start.7 = (bf16[80,1024]{1,0:T(8,128)(2,1)S(1)}, bf16[80,1024]{1,0:T(8,128)(2,1)S(1)}, u32[]{:S(2)}, u32[]{:S(2)}) collective-permute-start(bf16[80,1024]{1,0:T(8,128)(2,1)S(1)} %get-tuple-element.87), channel_id=1, source_target_pairs={{0,12},{4,8},{8,4},{12,0},{16,28},{20,24},{24,20},{28,16},{1,13},{... | collective-permute-start | bytes 491528 | tf_op jit(solution)/shard_map/ppermute | solution.py:407
  14.6 1.4 %collective-permute-start.14 = (bf16[80,512]{1,0:T(8,128)(2,1)S(1)}, bf16[80,512]{1,0:T(8,128)(2,1)S(1)}, u32[]{:S(2)}, u32[]{:S(2)}) collective-permute-start(bf16[80,512]{1,0:T(8,128)(2,1)S(1)} %get-tuple-element.90), channel_id=1, source_target_pairs={{0,24},{4,28},{8,16},{12,20},{16,8},{20,12},{24,0},{28,4},{1,25},{... | collective-permute-start | bytes 245768 | tf_op jit(solution)/shard_map/ppermute | solution.py:407
  16.0 6.9 %collective-permute-done.14 = bf16[80,512]{1,0:T(8,128)(2,1)S(1)} collective-permute-done((bf16[80,512]{1,0:T(8,128)(2,1)S(1)}, bf16[80,512]{1,0:T(8,128)(2,1)S(1)}, u32[]{:S(2)}, u32[]{:S(2)}) %collective-permute-start.14) | collective-permute-done | bytes 81952 | tf_op jit(solution)/shard_map/ppermute | solution.py:407
  22.9 7.1 %collective-permute-done.12 = bf16[80,512]{1,0:T(8,128)(2,1)S(1)} collective-permute-done((bf16[80,512]{1,0:T(8,128)(2,1)S(1)}, bf16[80,512]{1,0:T(8,128)(2,1)S(1)}, u32[]{:S(2)}, u32[]{:S(2)}) %collective-permute-start.12) | collective-permute-done | bytes 81952 | tf_op jit(solution)/shard_map/ppermute | solution.py:407
  30.1 3.7 %collective-permute-start.15 = (bf16[80,512]{1,0:T(8,128)(2,1)S(1)}, bf16[80,512]{1,0:T(8,128)(2,1)S(1)}, u32[]{:S(2)}, u32[]{:S(2)}) collective-permute-start(bf16[80,512]{1,0:T(8,128)(2,1)S(1)} %get-tuple-element.91), channel_id=1, source_target_pairs={{0,28},{4,24},{8,20},{12,16},{16,12},{20,8},{24,4},{28,0},{1,29},{... | collective-permute-start | bytes 245768 | tf_op jit(solution)/shard_map/ppermute | solution.py:407
  33.7 3.4 %collective-permute-done.15 = bf16[80,512]{1,0:T(8,128)(2,1)S(1)} collective-permute-done((bf16[80,512]{1,0:T(8,128)(2,1)S(1)}, bf16[80,512]{1,0:T(8,128)(2,1)S(1)}, u32[]{:S(2)}, u32[]{:S(2)}) %collective-permute-start.15) | collective-permute-done | bytes 81952 | tf_op jit(solution)/shard_map/ppermute | solution.py:407
  37.2 1.5 %collective-permute-start.13 = (bf16[160,512]{1,0:T(8,128)(2,1)S(1)}, bf16[160,512]{1,0:T(8,128)(2,1)S(1)}, u32[]{:S(2)}, u32[]{:S(2)}) collective-permute-start(bf16[160,512]{1,0:T(8,128)(2,1)S(1)} %constant_dynamic-update-slice_fusion.refs_7_), channel_id=1, source_target_pairs={{0,2},{1,3},{2,0},{3,1},{4,6},{5,7},{6,4},{7,5},{8,10},{9,11},{10,... | collective-permute-start | bytes 491528 | tf_op jit(solution)/shard_map/ppermute | solution.py:407
  39.9 2.6 %collective-permute-done.13.refs_8_ = bf16[160,512]{1,0:T(8,128)(2,1)S(1)} collective-permute-done((bf16[160,512]{1,0:T(8,128)(2,1)S(1)}, bf16[160,512]{1,0:T(8,128)(2,1)S(1)}, u32[]{:S(2)}, u32[]{:S(2)}) %collective-permute-start.13) | collective-permute-done | bytes 163872 | tf_op jit(solution)/shard_map/ppermute | solution.py:407
  42.5 1.8 %collective-permute-done.16.refs_10_ = bf16[160,512]{1,0:T(8,128)(2,1)S(1)} collective-permute-done((bf16[160,512]{1,0:T(8,128)(2,1)S(1)}, bf16[160,512]{1,0:T(8,128)(2,1)S(1)}, u32[]{:S(2)}, u32[]{:S(2)}) %collective-permute-start.16) | collective-permute-done | bytes 163872 | tf_op jit(solution)/shard_map/ppermute | solution.py:407
  44.9 3.9 %mixer_open_a.1 = (bf16[512,384]{1,0:T(8,128)(2,1)S(1)}, f32[8,384]{1,0:T(8,128)S(1)}, f32[8,384]{1,0:T(8,128)S(1)}, f32[8,384]{1,0:T(8,128)S(1)}, bf16[384,128]...) custom-call(s32[2]{0:T(128)S(1)} %pad_add_fusion.ids_ref, ...), custom_call_target="tpu_custom_call" | custom-call | flops 1000000000 | tf_op jit(solution)/shard_map/mixer_open_a/pallas_call | solution.py:47
  48.8 3.0 %mixer_open_b.1 = (bf16[512,384]{1,0:T(8,128)(2,1)S(1)}, bf16[544,128]{1,0:T(8,128)(2,1)S(1)}, bf16[544,128]{1,0:T(8,128)(2,1)S(1)}, bf16[1,2048,1280]{2,1,0:T(8,128)(2,1)S(1)}) custom-call(s32[2]{0:T(128)S(1)} %pad_add_fusion.ids_ref, bf16[1024,384]{1,0:T(8,128)(2,1)S(1)} %get-tuple-element.60.x_ref, f32[4,1024]{1,0:T(4,128)S(1)} %get-tuple-element.61.tx_ref, ...), custom_call_target="tpu_custom_call" | custom-call | flops 750000000 | tf_op jit(solution)/shard_map/mixer_open_b/pallas_call | solution.py:47
  51.9 7.8 %gate_up.1 = (bf16[320,1280]{1,0:T(8,128)(2,1)S(1)}, bf16[320,1280]{1,0:T(8,128)(2,1)S(1)}, bf16[1,1280,2048]{2,1,0:T(8,128)(2,1)S(1)}, bf16[1024,384]{1,0:T(8,128)(2,1)S(1)}) custom-call(s32[2]{0:T(128)S(1)} %pad_add_fusion.ids_ref, bf16[80,2048]{1,0:T(8,128)(2,1)S(1)} %get-tuple-element.84.refs_0_, bf16[80,1024]{1,0:T(8,128)(2,1)S(1)} %collective-permute-done.5.refs_1_, ...), custom_call_target="tpu_custom_call" | custom-call | flops 2249999872 | tf_op jit(solution)/shard_map/gate_up/pallas_call | solution.py:47
  59.7 2.4 %down_near.1 = (bf16[320,1024]{1,0:T(8,128)(2,1)S(1)}, bf16[320,1024]{1,0:T(8,128)(2,1)S(1)}) custom-call(s32[2]{0:T(128)S(1)} %pad_add_fusion.ids_ref, bf16[320,1280]{1,0:T(8,128)(2,1)S(1)} %get-tuple-element.97.h_ref, bf16[1,1280,2048]{2,1,0:T(8,128)(2,1)S(1)} %get-tuple-element.98.w_ref), custom_call_target="tpu_custom_call" | custom-call | flops 500000000 | tf_op jit(solution)/shard_map/down_near/pallas_call | solution.py:47
  62.7 2.4 %down_far.1 = (bf16[320,1024]{1,0:T(8,128)(2,1)S(1)}, bf16[320,1024]{1,0:T(8,128)(2,1)S(1)}) custom-call(s32[2]{0:T(128)S(1)} %pad_add_fusion.ids_ref, bf16[320,1280]{1,0:T(8,128)(2,1)S(1)} %get-tuple-element.107.h_ref, bf16[1,1280,2048]{2,1,0:T(8,128)(2,1)S(1)} %get-tuple-element.98.w_ref), custom_call_target="tpu_custom_call" | custom-call | flops 500000000 | tf_op jit(solution)/shard_map/down_far/pallas_call | solution.py:47
  65.3 6.0 %collective-permute-done.1.recv_ref.pair_ref = bf16[544,128]{1,0:T(8,128)(2,1)S(1)} collective-permute-done((bf16[544,128]{1,0:T(8,128)(2,1)S(1)}, bf16[544,128]{1,0:T(8,128)(2,1)S(1)}, u32[]{:S(2)}, u32[]{:S(2)}) %collective-permute-start.1) | collective-permute-done | bytes 139296 | tf_op jit(solution)/shard_map/ppermute | solution.py:407
  72.2 5.1 %collective-permute-done.2.recv_ref = bf16[544,128]{1,0:T(8,128)(2,1)S(1)} collective-permute-done((bf16[544,128]{1,0:T(8,128)(2,1)S(1)}, bf16[544,128]{1,0:T(8,128)(2,1)S(1)}, u32[]{:S(2)}, u32[]{:S(2)}) %collective-permute-start.2) | collective-permute-done | bytes 139296 | tf_op jit(solution)/shard_map/ppermute | solution.py:407
  77.9 3.5 %collective-permute-start.3 = (bf16[544,128]{1,0:T(8,128)(2,1)S(1)}, bf16[544,128]{1,0:T(8,128)(2,1)S(1)}, u32[]{:S(2)}, u32[]{:S(2)}) collective-permute-start(bf16[544,128]{1,0:T(8,128)(2,1)S(1)} %get-tuple-element.77), channel_id=1, source_target_pairs={{0,16},{4,20},{8,24},{12,28},{1,17},{5,21},{9,25},{13,29},{2,18},{... | collective-permute-start | bytes 417800 | tf_op jit(solution)/shard_map/ppermute | solution.py:776
  82.2 1.5 %collective-permute-start.22 = (bf16[80,1024]{1,0:T(8,128)(2,1)S(1)}, bf16[80,1024]{1,0:T(8,128)(2,1)S(1)}, u32[]{:S(2)}, u32[]{:S(2)}) collective-permute-start(bf16[80,1024]{1,0:T(8,128)(2,1)S(1)} %get-tuple-element.102), channel_id=1, source_target_pairs={{0,4},{4,0},{8,12},{12,8},{16,20},{20,16},{24,28},{28,24},{1,5},{5... | collective-permute-start | bytes 491528 | tf_op jit(solution)/shard_map/ppermute | solution.py:407
  83.7 1.7 %collective-permute-start.23 = (bf16[80,1024]{1,0:T(8,128)(2,1)S(1)}, bf16[80,1024]{1,0:T(8,128)(2,1)S(1)}, u32[]{:S(2)}, u32[]{:S(2)}) collective-permute-start(bf16[80,1024]{1,0:T(8,128)(2,1)S(1)} %get-tuple-element.103), channel_id=1, source_target_pairs={{0,8},{4,12},{8,0},{12,4},{16,24},{20,28},{24,16},{28,20},{1,9},{5... | collective-permute-start | bytes 491528 | tf_op jit(solution)/shard_map/ppermute | solution.py:407
  86.4 1.6 %collective-permute-start.27 = (bf16[160,512]{1,0:T(8,128)(2,1)S(1)}, bf16[160,512]{1,0:T(8,128)(2,1)S(1)}, u32[]{:S(2)}, u32[]{:S(2)}) collective-permute-start(bf16[160,512]{1,0:T(8,128)(2,1)S(1)} %get-tuple-element.111), channel_id=1, source_target_pairs={{0,2},{1,3},{2,0},{3,1},{4,6},{5,7},{6,4},{7,5},{8,10},{9,11},{10,... | collective-permute-start | bytes 491528 | tf_op jit(solution)/shard_map/ppermute | solution.py:407
  89.2 1.7 %collective-permute-start.4 = (bf16[512,128]{1,0:T(8,128)(2,1)S(1)}, bf16[512,128]{1,0:T(8,128)(2,1)S(1)}, u32[]{:S(2)}, u32[]{:S(2)}) collective-permute-start(bf16[512,128]{1,0:T(8,128)(2,1)S(1)} %get-tuple-element.79), channel_id=1, source_target_pairs={{0,4},{4,0},{8,12},{12,8},{16,20},{20,16},{24,28},{28,24},{1,5},{5... | collective-permute-start | bytes 393224 | tf_op jit(solution)/shard_map/ppermute | solution.py:407
  90.9 1.3 %collective-permute-done.24.refs_3_ = bf16[80,1024]{1,0:T(8,128)(2,1)S(1)} collective-permute-done((bf16[80,1024]{1,0:T(8,128)(2,1)S(1)}, bf16[80,1024]{1,0:T(8,128)(2,1)S(1)}, u32[]{:S(2)}, u32[]{:S(2)}) %collective-permute-start.24) | collective-permute-done | bytes 163872 | tf_op jit(solution)/shard_map/ppermute | solution.py:407
  93.4 1.6 %collective-permute-start.25 = (bf16[160,512]{1,0:T(8,128)(2,1)S(1)}, bf16[160,512]{1,0:T(8,128)(2,1)S(1)}, u32[]{:S(2)}, u32[]{:S(2)}) collective-permute-start(bf16[160,512]{1,0:T(8,128)(2,1)S(1)} %get-tuple-element.106), channel_id=1, source_target_pairs={{0,2},{1,3},{2,0},{3,1},{4,6},{5,7},{6,4},{7,5},{8,10},{9,11},{10,... | collective-permute-start | bytes 491528 | tf_op jit(solution)/shard_map/ppermute | solution.py:407
  96.7 2.4 %collective-permute-start.29 = (bf16[80,512]{1,0:T(8,128)(2,1)S(1)}, bf16[80,512]{1,0:T(8,128)(2,1)S(1)}, u32[]{:S(2)}, u32[]{:S(2)}) collective-permute-start(bf16[80,512]{1,0:T(8,128)(2,1)S(1)} %get-tuple-element.113), channel_id=1, source_target_pairs={{0,20},{4,16},{8,28},{12,24},{16,4},{20,0},{24,12},{28,8},{1,21},{... | collective-permute-start | bytes 245768 | tf_op jit(solution)/shard_map/ppermute | solution.py:407
  99.7 3.5 %collective-permute-start.31 = (bf16[80,512]{1,0:T(8,128)(2,1)S(1)}, bf16[80,512]{1,0:T(8,128)(2,1)S(1)}, u32[]{:S(2)}, u32[]{:S(2)}) collective-permute-start(bf16[80,512]{1,0:T(8,128)(2,1)S(1)} %get-tuple-element.116), channel_id=1, source_target_pairs={{0,24},{4,28},{8,16},{12,20},{16,8},{20,12},{24,0},{28,4},{1,25},{... | collective-permute-start | bytes 245768 | tf_op jit(solution)/shard_map/ppermute | solution.py:407
  103.9 3.9 %mixer_close.1 = bf16[1024,384]{1,0:T(8,128)(2,1)} custom-call(s32[2]{0:T(128)S(1)} %pad_add_fusion.ids_ref, bf16[512,128]{1,0:T(8,128)(2,1)S(1)} %get-tuple-element.78.keep_ref, bf16[512,128]{1,0:T(8,128)(2,1)S(1)} %collective-permute-done.4.recv_ref, bf16[512,384]{1,0:T(8,128)(2,1)S(1)} %get-tuple-element.80.xa_ref, ...), custom_call_target="tpu_custom_call" | custom-call | flops 1500000000 | tf_op jit(solution)/shard_map/mixer_close/pallas_call | solution.py:55
  109.1 1.4 %collective-permute-done.32.refs_4_ = bf16[80,512]{1,0:T(8,128)(2,1)S(1)} collective-permute-done((bf16[80,512]{1,0:T(8,128)(2,1)S(1)}, bf16[80,512]{1,0:T(8,128)(2,1)S(1)}, u32[]{:S(2)}, u32[]{:S(2)}) %collective-permute-start.32) | collective-permute-done | bytes 81952 | tf_op jit(solution)/shard_map/ppermute | solution.py:407
  110.4 1.7 %final_combine.1 = bf16[160,512]{1,0:T(8,128)(2,1)} custom-call(s32[2]{0:T(128)S(1)} %pad_add_fusion.ids_ref, f32[160,8]{1,0:T(8,128)S(1)} %get-tuple-element.96.table_ref, f32[160,512]{1,0:T(8,128)S(1)} %get-tuple-element.105.keep_ref, bf16[160,512]{1,0:T(8,128)(2,1)S(1)} %collective-permute-done.25.refs_0_, ...), custom_call_target="tpu_custom_call" | custom-call | flops 250000000 | tf_op jit(solution)/shard_map/final_combine/pallas_call | solution.py:47
  (55 shorter events, 12.5 us)
Async XLA Ops:
  3.6 11.1 %collective-permute-start.11 = (bf16[80,512]{1,0:T(8,128)(2,1)S(1)}, bf16[80,512]{1,0:T(8,128)(2,1)S(1)}, u32[]{:S(2)}, u32[]{:S(2)}) collective-permute-start(bf16[80,512]{1,0:T(8,128)(2,1)S(1)} %get-tuple-element.88), channel_id=1, source_target_pairs={{0,16},{4,20},{8,24},{12,28},{16,0},{20,4},{24,8},{28,12},{1,17},{... | collective-permute-start | bytes 245768 | tf_op jit(solution)/shard_map/ppermute | solution.py:407
  7.7 31.0 %collective-permute-start = (bf16[16,1280]{1,0:T(8,128)(2,1)S(1)}, bf16[16,1280]{1,0:T(8,128)(2,1)S(1)}, u32[]{:S(2)}, u32[]{:S(2)}) collective-permute-start(bf16[16,1280]{1,0:T(8,128)(2,1)S(1)} %get-tuple-element.62), channel_id=1, source_target_pairs={{0,4},{4,8},{8,12},{12,16},{16,20},{20,24},{24,28},{1,5},{5,9},{9,... | collective-permute-start | bytes 122888 | tf_op jit(solution)/shard_map/ppermute | solution.py:738
  11.1 28.2 %collective-permute-start.5 = (bf16[80,1024]{1,0:T(8,128)(2,1)S(1)}, bf16[80,1024]{1,0:T(8,128)(2,1)S(1)}, u32[]{:S(2)}, u32[]{:S(2)}) collective-permute-start(bf16[80,1024]{1,0:T(8,128)(2,1)S(1)} %get-tuple-element.85), channel_id=1, source_target_pairs={{0,4},{4,0},{8,12},{12,8},{16,20},{20,16},{24,28},{28,24},{1,5},{5... | collective-permute-start | bytes 491528 | tf_op jit(solution)/shard_map/ppermute | solution.py:407
  12.7 26.6 %collective-permute-start.6 = (bf16[80,1024]{1,0:T(8,128)(2,1)S(1)}, bf16[80,1024]{1,0:T(8,128)(2,1)S(1)}, u32[]{:S(2)}, u32[]{:S(2)}) collective-permute-start(bf16[80,1024]{1,0:T(8,128)(2,1)S(1)} %get-tuple-element.86), channel_id=1, source_target_pairs={{0,8},{4,12},{8,0},{12,4},{16,24},{20,28},{24,16},{28,20},{1,9},{5... | collective-permute-start | bytes 491528 | tf_op jit(solution)/shard_map/ppermute | solution.py:407
  12.8 27.0 %collective-permute-start.7 = (bf16[80,1024]{1,0:T(8,128)(2,1)S(1)}, bf16[80,1024]{1,0:T(8,128)(2,1)S(1)}, u32[]{:S(2)}, u32[]{:S(2)}) collective-permute-start(bf16[80,1024]{1,0:T(8,128)(2,1)S(1)} %get-tuple-element.87), channel_id=1, source_target_pairs={{0,12},{4,8},{8,4},{12,0},{16,28},{20,24},{24,20},{28,16},{1,13},{... | collective-permute-start | bytes 491528 | tf_op jit(solution)/shard_map/ppermute | solution.py:407
  14.6 8.3 %collective-permute-start.14 = (bf16[80,512]{1,0:T(8,128)(2,1)S(1)}, bf16[80,512]{1,0:T(8,128)(2,1)S(1)}, u32[]{:S(2)}, u32[]{:S(2)}) collective-permute-start(bf16[80,512]{1,0:T(8,128)(2,1)S(1)} %get-tuple-element.90), channel_id=1, source_target_pairs={{0,24},{4,28},{8,16},{12,20},{16,8},{20,12},{24,0},{28,4},{1,25},{... | collective-permute-start | bytes 245768 | tf_op jit(solution)/shard_map/ppermute | solution.py:407
  22.9 7.1 %collective-permute-start.12 = (bf16[80,512]{1,0:T(8,128)(2,1)S(1)}, bf16[80,512]{1,0:T(8,128)(2,1)S(1)}, u32[]{:S(2)}, u32[]{:S(2)}) collective-permute-start(bf16[80,512]{1,0:T(8,128)(2,1)S(1)} %get-tuple-element.89), channel_id=1, source_target_pairs={{0,20},{4,16},{8,28},{12,24},{16,4},{20,0},{24,12},{28,8},{1,21},{... | collective-permute-start | bytes 245768 | tf_op jit(solution)/shard_map/ppermute | solution.py:407
  30.1 7.1 %collective-permute-start.15 = (bf16[80,512]{1,0:T(8,128)(2,1)S(1)}, bf16[80,512]{1,0:T(8,128)(2,1)S(1)}, u32[]{:S(2)}, u32[]{:S(2)}) collective-permute-start(bf16[80,512]{1,0:T(8,128)(2,1)S(1)} %get-tuple-element.91), channel_id=1, source_target_pairs={{0,28},{4,24},{8,20},{12,16},{16,12},{20,8},{24,4},{28,0},{1,29},{... | collective-permute-start | bytes 245768 | tf_op jit(solution)/shard_map/ppermute | solution.py:407
  37.2 5.3 %collective-permute-start.13 = (bf16[160,512]{1,0:T(8,128)(2,1)S(1)}, bf16[160,512]{1,0:T(8,128)(2,1)S(1)}, u32[]{:S(2)}, u32[]{:S(2)}) collective-permute-start(bf16[160,512]{1,0:T(8,128)(2,1)S(1)} %constant_dynamic-update-slice_fusion.refs_7_), channel_id=1, source_target_pairs={{0,2},{1,3},{2,0},{3,1},{4,6},{5,7},{6,4},{7,5},{8,10},{9,11},{10,... | collective-permute-start | bytes 491528 | tf_op jit(solution)/shard_map/ppermute | solution.py:407
  38.7 5.5 %collective-permute-start.16 = (bf16[160,512]{1,0:T(8,128)(2,1)S(1)}, bf16[160,512]{1,0:T(8,128)(2,1)S(1)}, u32[]{:S(2)}, u32[]{:S(2)}) collective-permute-start(bf16[160,512]{1,0:T(8,128)(2,1)S(1)} %constant_dynamic-update-slice_fusion.2.refs_9_), channel_id=1, source_target_pairs={{0,2},{1,3},{2,0},{3,1},{4,6},{5,7},{6,4},{7,5},{8,10},{9,11},{10,... | collective-permute-start | bytes 491528 | tf_op jit(solution)/shard_map/ppermute | solution.py:407
  39.3 5.5 %collective-permute-start.19 = (bf16[160,512]{1,0:T(8,128)(2,1)S(1)}, bf16[160,512]{1,0:T(8,128)(2,1)S(1)}, u32[]{:S(2)}, u32[]{:S(2)}) collective-permute-start(bf16[160,512]{1,0:T(8,128)(2,1)S(1)} %constant_dynamic-update-slice_fusion.2.refs_9_), channel_id=1, source_target_pairs={{0,1},{1,0},{2,3},{3,2},{4,5},{5,4},{6,7},{7,6},{8,9},{9,8},{10,11... | collective-permute-start | bytes 491528 | tf_op jit(solution)/shard_map/ppermute | solution.py:407
  39.8 12.0 %collective-permute-start.8 = (bf16[80,1024]{1,0:T(8,128)(2,1)S(1)}, bf16[80,1024]{1,0:T(8,128)(2,1)S(1)}, u32[]{:S(2)}, u32[]{:S(2)}) collective-permute-start(bf16[80,1024]{1,0:T(8,128)(2,1)S(1)} %collective-permute-done.5.refs_1_), channel_id=1, source_target_pairs={{0,1},{1,0},{2,3},{3,2},{4,5},{5,4},{6,7},{7,6},{8,9},{9,8},{10,11... | collective-permute-start | bytes 491528 | tf_op jit(solution)/shard_map/ppermute | solution.py:407
  42.5 9.4 %collective-permute-start.9 = (bf16[80,1024]{1,0:T(8,128)(2,1)S(1)}, bf16[80,1024]{1,0:T(8,128)(2,1)S(1)}, u32[]{:S(2)}, u32[]{:S(2)}) collective-permute-start(bf16[80,1024]{1,0:T(8,128)(2,1)S(1)} %collective-permute-done.6.refs_2_), channel_id=1, source_target_pairs={{0,1},{1,0},{2,3},{3,2},{4,5},{5,4},{6,7},{7,6},{8,9},{9,8},{10,11... | collective-permute-start | bytes 491528 | tf_op jit(solution)/shard_map/ppermute | solution.py:407
  44.3 7.6 %collective-permute-start.10 = (bf16[80,1024]{1,0:T(8,128)(2,1)S(1)}, bf16[80,1024]{1,0:T(8,128)(2,1)S(1)}, u32[]{:S(2)}, u32[]{:S(2)}) collective-permute-start(bf16[80,1024]{1,0:T(8,128)(2,1)S(1)} %collective-permute-done.7.refs_3_), channel_id=1, source_target_pairs={{0,1},{1,0},{2,3},{3,2},{4,5},{5,4},{6,7},{7,6},{8,9},{9,8},{10,11... | collective-permute-start | bytes 491528 | tf_op jit(solution)/shard_map/ppermute | solution.py:407
  44.3 7.6 %collective-permute-start.18 = (bf16[160,512]{1,0:T(8,128)(2,1)S(1)}, bf16[160,512]{1,0:T(8,128)(2,1)S(1)}, u32[]{:S(2)}, u32[]{:S(2)}) collective-permute-start(bf16[160,512]{1,0:T(8,128)(2,1)S(1)} %collective-permute-done.13.refs_8_), channel_id=1, source_target_pairs={{0,1},{1,0},{2,3},{3,2},{4,5},{5,4},{6,7},{7,6},{8,9},{9,8},{10,11... | collective-permute-start | bytes 491528 | tf_op jit(solution)/shard_map/ppermute | solution.py:407
  44.8 7.1 %collective-permute-start.20 = (bf16[160,512]{1,0:T(8,128)(2,1)S(1)}, bf16[160,512]{1,0:T(8,128)(2,1)S(1)}, u32[]{:S(2)}, u32[]{:S(2)}) collective-permute-start(bf16[160,512]{1,0:T(8,128)(2,1)S(1)} %collective-permute-done.16.refs_10_), channel_id=1, source_target_pairs={{0,1},{1,0},{2,3},{3,2},{4,5},{5,4},{6,7},{7,6},{8,9},{9,8},{10,11... | collective-permute-start | bytes 491528 | tf_op jit(solution)/shard_map/ppermute | solution.py:407
  62.2 19.3 %collective-permute-start.21 = (bf16[320,1024]{1,0:T(8,128)(2,1)S(1)}, bf16[320,1024]{1,0:T(8,128)(2,1)S(1)}, u32[]{:S(2)}, u32[]{:S(2)}) collective-permute-start(bf16[320,1024]{1,0:T(8,128)(2,1)S(1)} %get-tuple-element.100), channel_id=1, source_target_pairs={{0,1},{1,0},{2,3},{3,2},{4,5},{5,4},{6,7},{7,6},{8,9},{9,8},{10,11... | collective-permute-start | bytes 1966088 | tf_op jit(solution)/shard_map/ppermute | solution.py:407
  65.1 20.6 %collective-permute-start.26 = (bf16[320,1024]{1,0:T(8,128)(2,1)S(1)}, bf16[320,1024]{1,0:T(8,128)(2,1)S(1)}, u32[]{:S(2)}, u32[]{:S(2)}) collective-permute-start(bf16[320,1024]{1,0:T(8,128)(2,1)S(1)} %get-tuple-element.109), channel_id=1, source_target_pairs={{0,1},{1,0},{2,3},{3,2},{4,5},{5,4},{6,7},{7,6},{8,9},{9,8},{10,11... | collective-permute-start | bytes 1966088 | tf_op jit(solution)/shard_map/ppermute | solution.py:407
  65.3 6.0 %collective-permute-start.1 = (bf16[544,128]{1,0:T(8,128)(2,1)S(1)}, bf16[544,128]{1,0:T(8,128)(2,1)S(1)}, u32[]{:S(2)}, u32[]{:S(2)}) collective-permute-start(bf16[544,128]{1,0:T(8,128)(2,1)S(1)} %get-tuple-element.74), channel_id=1, source_target_pairs={{0,4},{4,0},{8,12},{12,8},{16,20},{20,16},{24,28},{28,24},{1,5},{5... | collective-permute-start | bytes 417800 | tf_op jit(solution)/shard_map/ppermute | solution.py:407
  71.9 5.4 %collective-permute-start.2 = (bf16[544,128]{1,0:T(8,128)(2,1)S(1)}, bf16[544,128]{1,0:T(8,128)(2,1)S(1)}, u32[]{:S(2)}, u32[]{:S(2)}) collective-permute-start(bf16[544,128]{1,0:T(8,128)(2,1)S(1)} %state_pair.1.mine_ref), channel_id=1, source_target_pairs={{0,8},{4,12},{8,0},{12,4},{16,24},{20,28},{24,16},{28,20},{1,9},{5... | collective-permute-start | bytes 417800 | tf_op jit(solution)/shard_map/ppermute | solution.py:407
  77.9 10.1 %collective-permute-start.3 = (bf16[544,128]{1,0:T(8,128)(2,1)S(1)}, bf16[544,128]{1,0:T(8,128)(2,1)S(1)}, u32[]{:S(2)}, u32[]{:S(2)}) collective-permute-start(bf16[544,128]{1,0:T(8,128)(2,1)S(1)} %get-tuple-element.77), channel_id=1, source_target_pairs={{0,16},{4,20},{8,24},{12,28},{1,17},{5,21},{9,25},{13,29},{2,18},{... | collective-permute-start | bytes 417800 | tf_op jit(solution)/shard_map/ppermute | solution.py:776
  82.2 7.0 %collective-permute-start.22 = (bf16[80,1024]{1,0:T(8,128)(2,1)S(1)}, bf16[80,1024]{1,0:T(8,128)(2,1)S(1)}, u32[]{:S(2)}, u32[]{:S(2)}) collective-permute-start(bf16[80,1024]{1,0:T(8,128)(2,1)S(1)} %get-tuple-element.102), channel_id=1, source_target_pairs={{0,4},{4,0},{8,12},{12,8},{16,20},{20,16},{24,28},{28,24},{1,5},{5... | collective-permute-start | bytes 491528 | tf_op jit(solution)/shard_map/ppermute | solution.py:407
  83.7 7.2 %collective-permute-start.23 = (bf16[80,1024]{1,0:T(8,128)(2,1)S(1)}, bf16[80,1024]{1,0:T(8,128)(2,1)S(1)}, u32[]{:S(2)}, u32[]{:S(2)}) collective-permute-start(bf16[80,1024]{1,0:T(8,128)(2,1)S(1)} %get-tuple-element.103), channel_id=1, source_target_pairs={{0,8},{4,12},{8,0},{12,4},{16,24},{20,28},{24,16},{28,20},{1,9},{5... | collective-permute-start | bytes 491528 | tf_op jit(solution)/shard_map/ppermute | solution.py:407
  85.4 6.7 %collective-permute-start.24 = (bf16[80,1024]{1,0:T(8,128)(2,1)S(1)}, bf16[80,1024]{1,0:T(8,128)(2,1)S(1)}, u32[]{:S(2)}, u32[]{:S(2)}) collective-permute-start(bf16[80,1024]{1,0:T(8,128)(2,1)S(1)} %get-tuple-element.104), channel_id=1, source_target_pairs={{0,12},{4,8},{8,4},{12,0},{16,28},{20,24},{24,20},{28,16},{1,13},{... | collective-permute-start | bytes 491528 | tf_op jit(solution)/shard_map/ppermute | solution.py:407
  86.4 8.5 %collective-permute-start.27 = (bf16[160,512]{1,0:T(8,128)(2,1)S(1)}, bf16[160,512]{1,0:T(8,128)(2,1)S(1)}, u32[]{:S(2)}, u32[]{:S(2)}) collective-permute-start(bf16[160,512]{1,0:T(8,128)(2,1)S(1)} %get-tuple-element.111), channel_id=1, source_target_pairs={{0,2},{1,3},{2,0},{3,1},{4,6},{5,7},{6,4},{7,5},{8,10},{9,11},{10,... | collective-permute-start | bytes 491528 | tf_op jit(solution)/shard_map/ppermute | solution.py:407
  88.0 11.1 %collective-permute-start.30 = (bf16[160,512]{1,0:T(8,128)(2,1)S(1)}, bf16[160,512]{1,0:T(8,128)(2,1)S(1)}, u32[]{:S(2)}, u32[]{:S(2)}) collective-permute-start(bf16[160,512]{1,0:T(8,128)(2,1)S(1)} %get-tuple-element.115), channel_id=1, source_target_pairs={{0,2},{1,3},{2,0},{3,1},{4,6},{5,7},{6,4},{7,5},{8,10},{9,11},{10,... | collective-permute-start | bytes 491528 | tf_op jit(solution)/shard_map/ppermute | solution.py:407
  89.2 14.0 %collective-permute-start.4 = (bf16[512,128]{1,0:T(8,128)(2,1)S(1)}, bf16[512,128]{1,0:T(8,128)(2,1)S(1)}, u32[]{:S(2)}, u32[]{:S(2)}) collective-permute-start(bf16[512,128]{1,0:T(8,128)(2,1)S(1)} %get-tuple-element.79), channel_id=1, source_target_pairs={{0,4},{4,0},{8,12},{12,8},{16,20},{20,16},{24,28},{28,24},{1,5},{5... | collective-permute-start | bytes 393224 | tf_op jit(solution)/shard_map/ppermute | solution.py:407
  93.4 17.1 %collective-permute-start.25 = (bf16[160,512]{1,0:T(8,128)(2,1)S(1)}, bf16[160,512]{1,0:T(8,128)(2,1)S(1)}, u32[]{:S(2)}, u32[]{:S(2)}) collective-permute-start(bf16[160,512]{1,0:T(8,128)(2,1)S(1)} %get-tuple-element.106), channel_id=1, source_target_pairs={{0,2},{1,3},{2,0},{3,1},{4,6},{5,7},{6,4},{7,5},{8,10},{9,11},{10,... | collective-permute-start | bytes 491528 | tf_op jit(solution)/shard_map/ppermute | solution.py:407
  95.5 12.3 %collective-permute-start.28 = (bf16[80,512]{1,0:T(8,128)(2,1)S(1)}, bf16[80,512]{1,0:T(8,128)(2,1)S(1)}, u32[]{:S(2)}, u32[]{:S(2)}) collective-permute-start(bf16[80,512]{1,0:T(8,128)(2,1)S(1)} %get-tuple-element.112), channel_id=1, source_target_pairs={{0,16},{4,20},{8,24},{12,28},{16,0},{20,4},{24,8},{28,12},{1,17},{... | collective-permute-start | bytes 245768 | tf_op jit(solution)/shard_map/ppermute | solution.py:407
  96.7 12.4 %collective-permute-start.29 = (bf16[80,512]{1,0:T(8,128)(2,1)S(1)}, bf16[80,512]{1,0:T(8,128)(2,1)S(1)}, u32[]{:S(2)}, u32[]{:S(2)}) collective-permute-start(bf16[80,512]{1,0:T(8,128)(2,1)S(1)} %get-tuple-element.113), channel_id=1, source_target_pairs={{0,20},{4,16},{8,28},{12,24},{16,4},{20,0},{24,12},{28,8},{1,21},{... | collective-permute-start | bytes 245768 | tf_op jit(solution)/shard_map/ppermute | solution.py:407
  99.7 9.4 %collective-permute-start.31 = (bf16[80,512]{1,0:T(8,128)(2,1)S(1)}, bf16[80,512]{1,0:T(8,128)(2,1)S(1)}, u32[]{:S(2)}, u32[]{:S(2)}) collective-permute-start(bf16[80,512]{1,0:T(8,128)(2,1)S(1)} %get-tuple-element.116), channel_id=1, source_target_pairs={{0,24},{4,28},{8,16},{12,20},{16,8},{20,12},{24,0},{28,4},{1,25},{... | collective-permute-start | bytes 245768 | tf_op jit(solution)/shard_map/ppermute | solution.py:407
  103.2 7.2 %collective-permute-start.32 = (bf16[80,512]{1,0:T(8,128)(2,1)S(1)}, bf16[80,512]{1,0:T(8,128)(2,1)S(1)}, u32[]{:S(2)}, u32[]{:S(2)}) collective-permute-start(bf16[80,512]{1,0:T(8,128)(2,1)S(1)} %get-tuple-element.117), channel_id=1, source_target_pairs={{0,28},{4,24},{8,20},{12,16},{16,12},{20,8},{24,4},{28,0},{1,29},{... | collective-permute-start | bytes 245768 | tf_op jit(solution)/shard_map/ppermute | solution.py:407
  (1 other events, 5.0 us)

commit v2 on v1

--- a/solution.py
+++ b/solution.py
@@ -189,7 +189,7 @@
     outs += [sds(a.shape, a.dtype) for a in mixer_args]
     return call(
         body,
-        "prep",
+        "pr",
         ids,
         tuple(map(in_hbm, (moe_rows, moe_gain, routes_t, logit_t, *mixer_args))),
         outs,
@@ -261,7 +261,7 @@
     vmem = pl.BlockSpec(memory_space=pltpu.VMEM)
     return call(
         body,
-        "gate_up",
+        "gu",
         ids,
         (*pieces, w_gate, w_up, in_hbm(w_down), in_hbm(z_in)),
         [sds((split, hidden), BF)] * 2 + [sds(w_down.shape, BF), sds(z_in.shape, BF)],
@@ -307,7 +307,7 @@
             ).astype(BF)
 
     outs = [sds((cap, y_count * width), BF)] * half
-    return call(body, "near_sum", ids, (keep, received), outs)
+    return call(body, "ns", ids, (keep, received), outs)
 
 
 def far_split(ids, keep, received, sizes):
@@ -325,7 +325,7 @@
                 ).astype(BF)
 
     outs = [sds((rows // 2, width), BF)] * (2 * y_count)
-    return call(body, "far_split", ids, (keep, received), outs)
+    return call(body, "fs", ids, (keep, received), outs)
 
 
 def far_sum(ids, parts, sizes, name):
@@ -375,7 +375,7 @@
             outs[j][...] = total.astype(outs[j].dtype)
 
     outs = [sds((tokens, width), F32)] + [sds((tokens, width), BF)] * (y_count - 1)
-    return call(body, "near_combine", ids, (table, *parts), outs)
+    return call(body, "nc", ids, (table, *parts), outs)
 
 
 def final_combine(ids, parts, near_keep, near_received, table, sizes):
@@ -395,7 +395,7 @@
 
     return call(
         body,
-        "final_combine",
+        "fc",
         ids,
         (table, near_keep, *near_received, *parts),
         [sds((tokens, width), BF)],
@@ -506,7 +506,7 @@
     ]
     return call(
         body,
-        "mixer_open_a",
+        "ma",
         ids,
         (x_in, dt_raw, rate_row, b_in, c_in, taps_x, taps_b, taps_c, rims, in_hbm(weight)),
         outs,
@@ -539,7 +539,7 @@
     outs = [sds((part, length), BF), sds(message.shape, BF), sds(message.shape, BF), sds(weight.shape, weight.dtype)]
     return call(
         body,
-        "mixer_open_b",
+        "mb",
         ids,
         (x_in, taps_x, rims, step, cum, b_t, message, in_hbm(weight)),
         outs,
@@ -565,7 +565,7 @@
         msg_ref[rows : rows + hp, :] = high
         msg_ref[rows + hp :, :] = low
 
-    return call(body, "state_pair", ids, (mine, received), [sds(mine.shape, BF)])[0]
+    return call(body, "sp", ids, (mine, received), [sds(mine.shape, BF)])[0]
 
 
 def state_round(ids, mine, received, carried, level, hb, hp):
@@ -594,7 +594,7 @@
             dec_ref[...] = jnp.where(upper, old_dec[...] * d_recv, old_dec[...])
 
     ins = (mine, received) if opening else (mine, received, *carried)
-    return call(body, f"state_round_{level}", ids, ins, outs)
+    return call(body, f"q{level}", ids, ins, outs)
 
 
 def state_finish(ids, mine, pair, carried, last, hb, hp):
@@ -610,7 +610,7 @@
         keep_ref[...] = jnp.where(odd, after, before).astype(BF)
 
     outs = [sds((rows, NSTATE), BF)] * 2
-    return call(body, "state_finish", ids, (mine, pair, *carried, last), outs)
+    return call(body, "sf", ids, (mine, pair, *carried, last), outs)
 
 
 def mixer_close(ids, keep, received, xs_parts, cum_parts, b_t, c_conv, z_in, gain_row, hb):
@@ -670,7 +670,7 @@
     vmem = pl.BlockSpec(memory_space=pltpu.VMEM)
     return call(
         body,
-        "mixer_close",
+        "mc",
         ids,
         (keep, received, *xs_parts, *cum_parts, b_t, c_conv, z_in, gain_row),
         [sds((rows, length), BF)],
@@ -780,9 +780,9 @@
     hid_near, hid_far, w_down, z_in = gate_up(
         ids, self_rows, near, near_other, far_sets, far_other, w_gate, w_up, w_down, z_in, sizes
     )
-    send_far, keep_far = down(ids, hid_far, w_down, sizes, "down_far")
+    send_far, keep_far = down(ids, hid_far, w_down, sizes, "df")
     recv_far = swap(send_far, "tp", 1)
-    send_near, keep_near = down(ids, hid_near, w_down, sizes, "down_near")
+    send_near, keep_near = down(ids, hid_near, w_down, sizes, "dn")
     recv_near = swap(send_near, "tp", 1)
     near_out = near_sum(ids, keep_near, recv_near, sizes)
     near_back = [near_out[0]] + [swap(near_out[k], "ep", k) for k in range(1, half)]
@@ -794,7 +794,7 @@
         far_parts = [far_keep] + [
             swap(value, "tp", 2 * (j + 1)) for j, value in enumerate(far_send)
         ]
-        far_out = far_sum(ids, far_parts, sizes, "far_sum_" + label)
+        far_out = far_sum(ids, far_parts, sizes, "t" + label)
         first = half + part * (half // 2)
         far_back += [swap(value, "ep", first + index) for index, value in enumerate(far_out)]
     outs = near_combine(ids, near_back, table, sizes)

time: 112 us -> 112 us (level)
  no operation moved by 1% of the time
where the time goes in v2:
time: 112 us
  starting transfers between devices  40.5 us (36%)
  waiting for transfers between devices  36.9 us (33%)
  Pallas kernels  33.7 us (30%)
    ppermute x31, waiting for transfers between devices, swap(): return lax.ppermute(value, axis, [(i, i ^ step) for i in range(count)])  36.9 us
    ppermute x31, starting transfers between devices, swap(): return lax.ppermute(value, axis, [(i, i ^ step) for i in range(count)])  33.6 us
    pallas_call x15, Pallas kernels, launch(): pl.pallas_call(body, in_specs=[pl.BlockSpec(memory_space=pltpu.SMEM)] + (...  29.8 us
    pallas_call x1, Pallas kernels, launch(): pl.pallas_call(body, grid_spec=pltpu.PrefetchScalarGridSpec(num_scalar_pr...  3.9 us
    ppermute x1, starting transfers between devices, block(): last = lax.ppermute(message, 'ep', [(i, i + top) for i in range(ep - top)])  3.53 us
    ppermute x1, starting transfers between devices, block(): rims = lax.ppermute(own_rims, 'ep', [(i, i + 1) for i in range(ep - 1)])  3.39 us
  transfers between devices with their start and end apart: 33, of which 10 were waited for; matrix products, arithmetic and copies ran while one was open for 0% of the time, Pallas kernels for 17%

profile of v2, /device:TPU:0, one launch (start us, length us, event | category | flops | bytes accessed | tf_op | source)
XLA Modules:
  0.0 112.1 jit_solution(13122766936276883166)
XLA Ops:
  0.7 2.8 %pr.1 = (bf16[80,2048]{1,0:T(8,128)(2,1)S(1)}, bf16[80,1024]{1,0:T(8,128)(2,1)S(1)}, bf16[80,1024]{1,0:T(8,128)(2,1)S(1)}, bf16[80,1024]{1,0:T(8,128)(2,1)S(1)},...) custom-call(s32[2]{0:T(128)S(1)} %pad_add_fusion.ids_ref, ...), custom_call_target="tpu_custom_call" | custom-call | flops 750000000 | tf_op jit(solution)/shard_map/pr/pallas_call | solution.py:47
  3.6 4.1 %collective-permute-start.11 = (bf16[80,512]{1,0:T(8,128)(2,1)S(1)}, bf16[80,512]{1,0:T(8,128)(2,1)S(1)}, u32[]{:S(2)}, u32[]{:S(2)}) collective-permute-start(bf16[80,512]{1,0:T(8,128)(2,1)S(1)} %get-tuple-element.88), channel_id=1, source_target_pairs={{0,16},{4,20},{8,24},{12,28},{16,0},{20,4},{24,8},{28,12},{1,17},{... | collective-permute-start | bytes 245768 | tf_op jit(solution)/shard_map/ppermute | solution.py:407
  7.7 3.4 %collective-permute-start = (bf16[16,1280]{1,0:T(8,128)(2,1)S(1)}, bf16[16,1280]{1,0:T(8,128)(2,1)S(1)}, u32[]{:S(2)}, u32[]{:S(2)}) collective-permute-start(bf16[16,1280]{1,0:T(8,128)(2,1)S(1)} %get-tuple-element.62), channel_id=1, source_target_pairs={{0,4},{4,8},{8,12},{12,16},{16,20},{20,24},{24,28},{1,5},{5,9},{9,... | collective-permute-start | bytes 122888 | tf_op jit(solution)/shard_map/ppermute | solution.py:738
  11.1 1.6 %collective-permute-start.5 = (bf16[80,1024]{1,0:T(8,128)(2,1)S(1)}, bf16[80,1024]{1,0:T(8,128)(2,1)S(1)}, u32[]{:S(2)}, u32[]{:S(2)}) collective-permute-start(bf16[80,1024]{1,0:T(8,128)(2,1)S(1)} %get-tuple-element.85), channel_id=1, source_target_pairs={{0,4},{4,0},{8,12},{12,8},{16,20},{20,16},{24,28},{28,24},{1,5},{5... | collective-permute-start | bytes 491528 | tf_op jit(solution)/shard_map/ppermute | solution.py:407
  12.8 1.8 %collective-permute-start.7 = (bf16[80,1024]{1,0:T(8,128)(2,1)S(1)}, bf16[80,1024]{1,0:T(8,128)(2,1)S(1)}, u32[]{:S(2)}, u32[]{:S(2)}) collective-permute-start(bf16[80,1024]{1,0:T(8,128)(2,1)S(1)} %get-tuple-element.87), channel_id=1, source_target_pairs={{0,12},{4,8},{8,4},{12,0},{16,28},{20,24},{24,20},{28,16},{1,13},{... | collective-permute-start | bytes 491528 | tf_op jit(solution)/shard_map/ppermute | solution.py:407
  14.6 1.4 %collective-permute-start.14 = (bf16[80,512]{1,0:T(8,128)(2,1)S(1)}, bf16[80,512]{1,0:T(8,128)(2,1)S(1)}, u32[]{:S(2)}, u32[]{:S(2)}) collective-permute-start(bf16[80,512]{1,0:T(8,128)(2,1)S(1)} %get-tuple-element.90), channel_id=1, source_target_pairs={{0,24},{4,28},{8,16},{12,20},{16,8},{20,12},{24,0},{28,4},{1,25},{... | collective-permute-start | bytes 245768 | tf_op jit(solution)/shard_map/ppermute | solution.py:407
  16.0 6.9 %collective-permute-done.14 = bf16[80,512]{1,0:T(8,128)(2,1)S(1)} collective-permute-done((bf16[80,512]{1,0:T(8,128)(2,1)S(1)}, bf16[80,512]{1,0:T(8,128)(2,1)S(1)}, u32[]{:S(2)}, u32[]{:S(2)}) %collective-permute-start.14) | collective-permute-done | bytes 81952 | tf_op jit(solution)/shard_map/ppermute | solution.py:407
  22.9 7.1 %collective-permute-done.12 = bf16[80,512]{1,0:T(8,128)(2,1)S(1)} collective-permute-done((bf16[80,512]{1,0:T(8,128)(2,1)S(1)}, bf16[80,512]{1,0:T(8,128)(2,1)S(1)}, u32[]{:S(2)}, u32[]{:S(2)}) %collective-permute-start.12) | collective-permute-done | bytes 81952 | tf_op jit(solution)/shard_map/ppermute | solution.py:407
  30.1 3.7 %collective-permute-start.15 = (bf16[80,512]{1,0:T(8,128)(2,1)S(1)}, bf16[80,512]{1,0:T(8,128)(2,1)S(1)}, u32[]{:S(2)}, u32[]{:S(2)}) collective-permute-start(bf16[80,512]{1,0:T(8,128)(2,1)S(1)} %get-tuple-element.91), channel_id=1, source_target_pairs={{0,28},{4,24},{8,20},{12,16},{16,12},{20,8},{24,4},{28,0},{1,29},{... | collective-permute-start | bytes 245768 | tf_op jit(solution)/shard_map/ppermute | solution.py:407
  33.7 3.4 %collective-permute-done.15 = bf16[80,512]{1,0:T(8,128)(2,1)S(1)} collective-permute-done((bf16[80,512]{1,0:T(8,128)(2,1)S(1)}, bf16[80,512]{1,0:T(8,128)(2,1)S(1)}, u32[]{:S(2)}, u32[]{:S(2)}) %collective-permute-start.15) | collective-permute-done | bytes 81952 | tf_op jit(solution)/shard_map/ppermute | solution.py:407
  37.2 1.5 %collective-permute-start.13 = (bf16[160,512]{1,0:T(8,128)(2,1)S(1)}, bf16[160,512]{1,0:T(8,128)(2,1)S(1)}, u32[]{:S(2)}, u32[]{:S(2)}) collective-permute-start(bf16[160,512]{1,0:T(8,128)(2,1)S(1)} %constant_dynamic-update-slice_fusion.refs_7_), channel_id=1, source_target_pairs={{0,2},{1,3},{2,0},{3,1},{4,6},{5,7},{6,4},{7,5},{8,10},{9,11},{10,... | collective-permute-start | bytes 491528 | tf_op jit(solution)/shard_map/ppermute | solution.py:407
  39.9 2.6 %collective-permute-done.13.refs_8_ = bf16[160,512]{1,0:T(8,128)(2,1)S(1)} collective-permute-done((bf16[160,512]{1,0:T(8,128)(2,1)S(1)}, bf16[160,512]{1,0:T(8,128)(2,1)S(1)}, u32[]{:S(2)}, u32[]{:S(2)}) %collective-permute-start.13) | collective-permute-done | bytes 163872 | tf_op jit(solution)/shard_map/ppermute | solution.py:407
  42.5 1.8 %collective-permute-done.16.refs_10_ = bf16[160,512]{1,0:T(8,128)(2,1)S(1)} collective-permute-done((bf16[160,512]{1,0:T(8,128)(2,1)S(1)}, bf16[160,512]{1,0:T(8,128)(2,1)S(1)}, u32[]{:S(2)}, u32[]{:S(2)}) %collective-permute-start.16) | collective-permute-done | bytes 163872 | tf_op jit(solution)/shard_map/ppermute | solution.py:407
  44.9 3.9 %ma.1 = (bf16[512,384]{1,0:T(8,128)(2,1)S(1)}, f32[8,384]{1,0:T(8,128)S(1)}, f32[8,384]{1,0:T(8,128)S(1)}, f32[8,384]{1,0:T(8,128)S(1)}, bf16[384,128]{1,0:T(8,1...) custom-call(s32[2]{0:T(128)S(1)} %pad_add_fusion.ids_ref, ...), custom_call_target="tpu_custom_call" | custom-call | flops 1000000000 | tf_op jit(solution)/shard_map/ma/pallas_call | solution.py:47
  48.8 3.0 %mb.1 = (bf16[512,384]{1,0:T(8,128)(2,1)S(1)}, bf16[544,128]{1,0:T(8,128)(2,1)S(1)}, bf16[544,128]{1,0:T(8,128)(2,1)S(1)}, bf16[1,2048,1280]{2,1,0:T(8,128)(2,1)S(1)}) custom-call(s32[2]{0:T(128)S(1)} %pad_add_fusion.ids_ref, bf16[1024,384]{1,0:T(8,128)(2,1)S(1)} %get-tuple-element.60.x_ref, f32[4,1024]{1,0:T(4,128)S(1)} %get-tuple-element.61.tx_ref, ...), custom_call_target="tpu_custom_call" | custom-call | flops 750000000 | tf_op jit(solution)/shard_map/mb/pallas_call | solution.py:47
  51.9 7.8 %gu.1 = (bf16[320,1280]{1,0:T(8,128)(2,1)S(1)}, bf16[320,1280]{1,0:T(8,128)(2,1)S(1)}, bf16[1,1280,2048]{2,1,0:T(8,128)(2,1)S(1)}, bf16[1024,384]{1,0:T(8,128)(2,1)S(1)}) custom-call(s32[2]{0:T(128)S(1)} %pad_add_fusion.ids_ref, bf16[80,2048]{1,0:T(8,128)(2,1)S(1)} %get-tuple-element.84.refs_0_, bf16[80,1024]{1,0:T(8,128)(2,1)S(1)} %collective-permute-done.5.refs_1_, ...), custom_call_target="tpu_custom_call" | custom-call | flops 2249999872 | tf_op jit(solution)/shard_map/gu/pallas_call | solution.py:47
  59.7 2.4 %dn.1 = (bf16[320,1024]{1,0:T(8,128)(2,1)S(1)}, bf16[320,1024]{1,0:T(8,128)(2,1)S(1)}) custom-call(s32[2]{0:T(128)S(1)} %pad_add_fusion.ids_ref, bf16[320,1280]{1,0:T(8,128)(2,1)S(1)} %get-tuple-element.97.h_ref, bf16[1,1280,2048]{2,1,0:T(8,128)(2,1)S(1)} %get-tuple-element.98.w_ref), custom_call_target="tpu_custom_call" | custom-call | flops 500000000 | tf_op jit(solution)/shard_map/dn/pallas_call | solution.py:47
  62.7 2.4 %df.1 = (bf16[320,1024]{1,0:T(8,128)(2,1)S(1)}, bf16[320,1024]{1,0:T(8,128)(2,1)S(1)}) custom-call(s32[2]{0:T(128)S(1)} %pad_add_fusion.ids_ref, bf16[320,1280]{1,0:T(8,128)(2,1)S(1)} %get-tuple-element.107.h_ref, bf16[1,1280,2048]{2,1,0:T(8,128)(2,1)S(1)} %get-tuple-element.98.w_ref), custom_call_target="tpu_custom_call" | custom-call | flops 500000000 | tf_op jit(solution)/shard_map/df/pallas_call | solution.py:47
  65.3 6.0 %collective-permute-done.1.recv_ref.pair_ref = bf16[544,128]{1,0:T(8,128)(2,1)S(1)} collective-permute-done((bf16[544,128]{1,0:T(8,128)(2,1)S(1)}, bf16[544,128]{1,0:T(8,128)(2,1)S(1)}, u32[]{:S(2)}, u32[]{:S(2)}) %collective-permute-start.1) | collective-permute-done | bytes 139296 | tf_op jit(solution)/shard_map/ppermute | solution.py:407
  72.2 5.1 %collective-permute-done.2.recv_ref = bf16[544,128]{1,0:T(8,128)(2,1)S(1)} collective-permute-done((bf16[544,128]{1,0:T(8,128)(2,1)S(1)}, bf16[544,128]{1,0:T(8,128)(2,1)S(1)}, u32[]{:S(2)}, u32[]{:S(2)}) %collective-permute-start.2) | collective-permute-done | bytes 139296 | tf_op jit(solution)/shard_map/ppermute | solution.py:407
  77.9 3.5 %collective-permute-start.3 = (bf16[544,128]{1,0:T(8,128)(2,1)S(1)}, bf16[544,128]{1,0:T(8,128)(2,1)S(1)}, u32[]{:S(2)}, u32[]{:S(2)}) collective-permute-start(bf16[544,128]{1,0:T(8,128)(2,1)S(1)} %get-tuple-element.77), channel_id=1, source_target_pairs={{0,16},{4,20},{8,24},{12,28},{1,17},{5,21},{9,25},{13,29},{2,18},{... | collective-permute-start | bytes 417800 | tf_op jit(solution)/shard_map/ppermute | solution.py:776
  82.2 1.5 %collective-permute-start.22 = (bf16[80,1024]{1,0:T(8,128)(2,1)S(1)}, bf16[80,1024]{1,0:T(8,128)(2,1)S(1)}, u32[]{:S(2)}, u32[]{:S(2)}) collective-permute-start(bf16[80,1024]{1,0:T(8,128)(2,1)S(1)} %get-tuple-element.102), channel_id=1, source_target_pairs={{0,4},{4,0},{8,12},{12,8},{16,20},{20,16},{24,28},{28,24},{1,5},{5... | collective-permute-start | bytes 491528 | tf_op jit(solution)/shard_map/ppermute | solution.py:407
  83.7 1.7 %collective-permute-start.23 = (bf16[80,1024]{1,0:T(8,128)(2,1)S(1)}, bf16[80,1024]{1,0:T(8,128)(2,1)S(1)}, u32[]{:S(2)}, u32[]{:S(2)}) collective-permute-start(bf16[80,1024]{1,0:T(8,128)(2,1)S(1)} %get-tuple-element.103), channel_id=1, source_target_pairs={{0,8},{4,12},{8,0},{12,4},{16,24},{20,28},{24,16},{28,20},{1,9},{5... | collective-permute-start | bytes 491528 | tf_op jit(solution)/shard_map/ppermute | solution.py:407
  86.4 1.6 %collective-permute-start.27 = (bf16[160,512]{1,0:T(8,128)(2,1)S(1)}, bf16[160,512]{1,0:T(8,128)(2,1)S(1)}, u32[]{:S(2)}, u32[]{:S(2)}) collective-permute-start(bf16[160,512]{1,0:T(8,128)(2,1)S(1)} %get-tuple-element.111), channel_id=1, source_target_pairs={{0,2},{1,3},{2,0},{3,1},{4,6},{5,7},{6,4},{7,5},{8,10},{9,11},{10,... | collective-permute-start | bytes 491528 | tf_op jit(solution)/shard_map/ppermute | solution.py:407
  89.2 1.7 %collective-permute-start.4 = (bf16[512,128]{1,0:T(8,128)(2,1)S(1)}, bf16[512,128]{1,0:T(8,128)(2,1)S(1)}, u32[]{:S(2)}, u32[]{:S(2)}) collective-permute-start(bf16[512,128]{1,0:T(8,128)(2,1)S(1)} %get-tuple-element.79), channel_id=1, source_target_pairs={{0,4},{4,0},{8,12},{12,8},{16,20},{20,16},{24,28},{28,24},{1,5},{5... | collective-permute-start | bytes 393224 | tf_op jit(solution)/shard_map/ppermute | solution.py:407
  90.9 1.3 %collective-permute-done.24.refs_3_ = bf16[80,1024]{1,0:T(8,128)(2,1)S(1)} collective-permute-done((bf16[80,1024]{1,0:T(8,128)(2,1)S(1)}, bf16[80,1024]{1,0:T(8,128)(2,1)S(1)}, u32[]{:S(2)}, u32[]{:S(2)}) %collective-permute-start.24) | collective-permute-done | bytes 163872 | tf_op jit(solution)/shard_map/ppermute | solution.py:407
  93.4 1.6 %collective-permute-start.25 = (bf16[160,512]{1,0:T(8,128)(2,1)S(1)}, bf16[160,512]{1,0:T(8,128)(2,1)S(1)}, u32[]{:S(2)}, u32[]{:S(2)}) collective-permute-start(bf16[160,512]{1,0:T(8,128)(2,1)S(1)} %get-tuple-element.106), channel_id=1, source_target_pairs={{0,2},{1,3},{2,0},{3,1},{4,6},{5,7},{6,4},{7,5},{8,10},{9,11},{10,... | collective-permute-start | bytes 491528 | tf_op jit(solution)/shard_map/ppermute | solution.py:407
  96.7 2.4 %collective-permute-start.29 = (bf16[80,512]{1,0:T(8,128)(2,1)S(1)}, bf16[80,512]{1,0:T(8,128)(2,1)S(1)}, u32[]{:S(2)}, u32[]{:S(2)}) collective-permute-start(bf16[80,512]{1,0:T(8,128)(2,1)S(1)} %get-tuple-element.113), channel_id=1, source_target_pairs={{0,20},{4,16},{8,28},{12,24},{16,4},{20,0},{24,12},{28,8},{1,21},{... | collective-permute-start | bytes 245768 | tf_op jit(solution)/shard_map/ppermute | solution.py:407
  99.7 3.5 %collective-permute-start.31 = (bf16[80,512]{1,0:T(8,128)(2,1)S(1)}, bf16[80,512]{1,0:T(8,128)(2,1)S(1)}, u32[]{:S(2)}, u32[]{:S(2)}) collective-permute-start(bf16[80,512]{1,0:T(8,128)(2,1)S(1)} %get-tuple-element.116), channel_id=1, source_target_pairs={{0,24},{4,28},{8,16},{12,20},{16,8},{20,12},{24,0},{28,4},{1,25},{... | collective-permute-start | bytes 245768 | tf_op jit(solution)/shard_map/ppermute | solution.py:407
  103.9 3.9 %mc.1 = bf16[1024,384]{1,0:T(8,128)(2,1)} custom-call(s32[2]{0:T(128)S(1)} %pad_add_fusion.ids_ref, bf16[512,128]{1,0:T(8,128)(2,1)S(1)} %get-tuple-element.78.keep_ref, bf16[512,128]{1,0:T(8,128)(2,1)S(1)} %collective-permute-done.4.recv_ref, bf16[512,384]{1,0:T(8,128)(2,1)S(1)} %get-tuple-element.80.xa_ref, bf16[512,384]{1,0:T(8,128)(2,1)S(1)} %get-tuple-element.81.xb_ref, ...), custom_call_target="tpu_custom_call" | custom-call | flops 1500000000 | tf_op jit(solution)/shard_map/mc/pallas_call | solution.py:55
  109.1 1.4 %collective-permute-done.32.refs_4_ = bf16[80,512]{1,0:T(8,128)(2,1)S(1)} collective-permute-done((bf16[80,512]{1,0:T(8,128)(2,1)S(1)}, bf16[80,512]{1,0:T(8,128)(2,1)S(1)}, u32[]{:S(2)}, u32[]{:S(2)}) %collective-permute-start.32) | collective-permute-done | bytes 81952 | tf_op jit(solution)/shard_map/ppermute | solution.py:407
  110.4 1.7 %fc.1 = bf16[160,512]{1,0:T(8,128)(2,1)} custom-call(s32[2]{0:T(128)S(1)} %pad_add_fusion.ids_ref, f32[160,8]{1,0:T(8,128)S(1)} %get-tuple-element.96.table_ref, f32[160,512]{1,0:T(8,128)S(1)} %get-tuple-element.105.keep_ref, bf16[160,512]{1,0:T(8,128)(2,1)S(1)} %collective-permute-done.25.refs_0_, bf16[80,512]{1,0:T(8,128)(2,1)S(1)} %collective-permute-done.28.refs_1_, ...), custom_call_target="tpu_custom_call" | custom-call | flops 250000000 | tf_op jit(solution)/shard_map/fc/pallas_call | solution.py:47
  (55 shorter events, 12.5 us)
Async XLA Ops:
  3.6 11.1 %collective-permute-start.11 = (bf16[80,512]{1,0:T(8,128)(2,1)S(1)}, bf16[80,512]{1,0:T(8,128)(2,1)S(1)}, u32[]{:S(2)}, u32[]{:S(2)}) collective-permute-start(bf16[80,512]{1,0:T(8,128)(2,1)S(1)} %get-tuple-element.88), channel_id=1, source_target_pairs={{0,16},{4,20},{8,24},{12,28},{16,0},{20,4},{24,8},{28,12},{1,17},{... | collective-permute-start | bytes 245768 | tf_op jit(solution)/shard_map/ppermute | solution.py:407
  7.7 31.0 %collective-permute-start = (bf16[16,1280]{1,0:T(8,128)(2,1)S(1)}, bf16[16,1280]{1,0:T(8,128)(2,1)S(1)}, u32[]{:S(2)}, u32[]{:S(2)}) collective-permute-start(bf16[16,1280]{1,0:T(8,128)(2,1)S(1)} %get-tuple-element.62), channel_id=1, source_target_pairs={{0,4},{4,8},{8,12},{12,16},{16,20},{20,24},{24,28},{1,5},{5,9},{9,... | collective-permute-start | bytes 122888 | tf_op jit(solution)/shard_map/ppermute | solution.py:738
  11.1 28.2 %collective-permute-start.5 = (bf16[80,1024]{1,0:T(8,128)(2,1)S(1)}, bf16[80,1024]{1,0:T(8,128)(2,1)S(1)}, u32[]{:S(2)}, u32[]{:S(2)}) collective-permute-start(bf16[80,1024]{1,0:T(8,128)(2,1)S(1)} %get-tuple-element.85), channel_id=1, source_target_pairs={{0,4},{4,0},{8,12},{12,8},{16,20},{20,16},{24,28},{28,24},{1,5},{5... | collective-permute-start | bytes 491528 | tf_op jit(solution)/shard_map/ppermute | solution.py:407
  12.7 26.6 %collective-permute-start.6 = (bf16[80,1024]{1,0:T(8,128)(2,1)S(1)}, bf16[80,1024]{1,0:T(8,128)(2,1)S(1)}, u32[]{:S(2)}, u32[]{:S(2)}) collective-permute-start(bf16[80,1024]{1,0:T(8,128)(2,1)S(1)} %get-tuple-element.86), channel_id=1, source_target_pairs={{0,8},{4,12},{8,0},{12,4},{16,24},{20,28},{24,16},{28,20},{1,9},{5... | collective-permute-start | bytes 491528 | tf_op jit(solution)/shard_map/ppermute | solution.py:407
  12.8 27.0 %collective-permute-start.7 = (bf16[80,1024]{1,0:T(8,128)(2,1)S(1)}, bf16[80,1024]{1,0:T(8,128)(2,1)S(1)}, u32[]{:S(2)}, u32[]{:S(2)}) collective-permute-start(bf16[80,1024]{1,0:T(8,128)(2,1)S(1)} %get-tuple-element.87), channel_id=1, source_target_pairs={{0,12},{4,8},{8,4},{12,0},{16,28},{20,24},{24,20},{28,16},{1,13},{... | collective-permute-start | bytes 491528 | tf_op jit(solution)/shard_map/ppermute | solution.py:407
  14.6 8.3 %collective-permute-start.14 = (bf16[80,512]{1,0:T(8,128)(2,1)S(1)}, bf16[80,512]{1,0:T(8,128)(2,1)S(1)}, u32[]{:S(2)}, u32[]{:S(2)}) collective-permute-start(bf16[80,512]{1,0:T(8,128)(2,1)S(1)} %get-tuple-element.90), channel_id=1, source_target_pairs={{0,24},{4,28},{8,16},{12,20},{16,8},{20,12},{24,0},{28,4},{1,25},{... | collective-permute-start | bytes 245768 | tf_op jit(solution)/shard_map/ppermute | solution.py:407
  22.9 7.1 %collective-permute-start.12 = (bf16[80,512]{1,0:T(8,128)(2,1)S(1)}, bf16[80,512]{1,0:T(8,128)(2,1)S(1)}, u32[]{:S(2)}, u32[]{:S(2)}) collective-permute-start(bf16[80,512]{1,0:T(8,128)(2,1)S(1)} %get-tuple-element.89), channel_id=1, source_target_pairs={{0,20},{4,16},{8,28},{12,24},{16,4},{20,0},{24,12},{28,8},{1,21},{... | collective-permute-start | bytes 245768 | tf_op jit(solution)/shard_map/ppermute | solution.py:407
  30.1 7.1 %collective-permute-start.15 = (bf16[80,512]{1,0:T(8,128)(2,1)S(1)}, bf16[80,512]{1,0:T(8,128)(2,1)S(1)}, u32[]{:S(2)}, u32[]{:S(2)}) collective-permute-start(bf16[80,512]{1,0:T(8,128)(2,1)S(1)} %get-tuple-element.91), channel_id=1, source_target_pairs={{0,28},{4,24},{8,20},{12,16},{16,12},{20,8},{24,4},{28,0},{1,29},{... | collective-permute-start | bytes 245768 | tf_op jit(solution)/shard_map/ppermute | solution.py:407
  37.2 5.3 %collective-permute-start.13 = (bf16[160,512]{1,0:T(8,128)(2,1)S(1)}, bf16[160,512]{1,0:T(8,128)(2,1)S(1)}, u32[]{:S(2)}, u32[]{:S(2)}) collective-permute-start(bf16[160,512]{1,0:T(8,128)(2,1)S(1)} %constant_dynamic-update-slice_fusion.refs_7_), channel_id=1, source_target_pairs={{0,2},{1,3},{2,0},{3,1},{4,6},{5,7},{6,4},{7,5},{8,10},{9,11},{10,... | collective-permute-start | bytes 491528 | tf_op jit(solution)/shard_map/ppermute | solution.py:407
  38.7 5.5 %collective-permute-start.16 = (bf16[160,512]{1,0:T(8,128)(2,1)S(1)}, bf16[160,512]{1,0:T(8,128)(2,1)S(1)}, u32[]{:S(2)}, u32[]{:S(2)}) collective-permute-start(bf16[160,512]{1,0:T(8,128)(2,1)S(1)} %constant_dynamic-update-slice_fusion.2.refs_9_), channel_id=1, source_target_pairs={{0,2},{1,3},{2,0},{3,1},{4,6},{5,7},{6,4},{7,5},{8,10},{9,11},{10,... | collective-permute-start | bytes 491528 | tf_op jit(solution)/shard_map/ppermute | solution.py:407
  39.3 5.5 %collective-permute-start.19 = (bf16[160,512]{1,0:T(8,128)(2,1)S(1)}, bf16[160,512]{1,0:T(8,128)(2,1)S(1)}, u32[]{:S(2)}, u32[]{:S(2)}) collective-permute-start(bf16[160,512]{1,0:T(8,128)(2,1)S(1)} %constant_dynamic-update-slice_fusion.2.refs_9_), channel_id=1, source_target_pairs={{0,1},{1,0},{2,3},{3,2},{4,5},{5,4},{6,7},{7,6},{8,9},{9,8},{10,11... | collective-permute-start | bytes 491528 | tf_op jit(solution)/shard_map/ppermute | solution.py:407
  39.8 12.0 %collective-permute-start.8 = (bf16[80,1024]{1,0:T(8,128)(2,1)S(1)}, bf16[80,1024]{1,0:T(8,128)(2,1)S(1)}, u32[]{:S(2)}, u32[]{:S(2)}) collective-permute-start(bf16[80,1024]{1,0:T(8,128)(2,1)S(1)} %collective-permute-done.5.refs_1_), channel_id=1, source_target_pairs={{0,1},{1,0},{2,3},{3,2},{4,5},{5,4},{6,7},{7,6},{8,9},{9,8},{10,11... | collective-permute-start | bytes 491528 | tf_op jit(solution)/shard_map/ppermute | solution.py:407
  42.5 9.4 %collective-permute-start.9 = (bf16[80,1024]{1,0:T(8,128)(2,1)S(1)}, bf16[80,1024]{1,0:T(8,128)(2,1)S(1)}, u32[]{:S(2)}, u32[]{:S(2)}) collective-permute-start(bf16[80,1024]{1,0:T(8,128)(2,1)S(1)} %collective-permute-done.6.refs_2_), channel_id=1, source_target_pairs={{0,1},{1,0},{2,3},{3,2},{4,5},{5,4},{6,7},{7,6},{8,9},{9,8},{10,11... | collective-permute-start | bytes 491528 | tf_op jit(solution)/shard_map/ppermute | solution.py:407
  44.3 7.6 %collective-permute-start.10 = (bf16[80,1024]{1,0:T(8,128)(2,1)S(1)}, bf16[80,1024]{1,0:T(8,128)(2,1)S(1)}, u32[]{:S(2)}, u32[]{:S(2)}) collective-permute-start(bf16[80,1024]{1,0:T(8,128)(2,1)S(1)} %collective-permute-done.7.refs_3_), channel_id=1, source_target_pairs={{0,1},{1,0},{2,3},{3,2},{4,5},{5,4},{6,7},{7,6},{8,9},{9,8},{10,11... | collective-permute-start | bytes 491528 | tf_op jit(solution)/shard_map/ppermute | solution.py:407
  44.3 7.6 %collective-permute-start.18 = (bf16[160,512]{1,0:T(8,128)(2,1)S(1)}, bf16[160,512]{1,0:T(8,128)(2,1)S(1)}, u32[]{:S(2)}, u32[]{:S(2)}) collective-permute-start(bf16[160,512]{1,0:T(8,128)(2,1)S(1)} %collective-permute-done.13.refs_8_), channel_id=1, source_target_pairs={{0,1},{1,0},{2,3},{3,2},{4,5},{5,4},{6,7},{7,6},{8,9},{9,8},{10,11... | collective-permute-start | bytes 491528 | tf_op jit(solution)/shard_map/ppermute | solution.py:407
  44.8 7.1 %collective-permute-start.20 = (bf16[160,512]{1,0:T(8,128)(2,1)S(1)}, bf16[160,512]{1,0:T(8,128)(2,1)S(1)}, u32[]{:S(2)}, u32[]{:S(2)}) collective-permute-start(bf16[160,512]{1,0:T(8,128)(2,1)S(1)} %collective-permute-done.16.refs_10_), channel_id=1, source_target_pairs={{0,1},{1,0},{2,3},{3,2},{4,5},{5,4},{6,7},{7,6},{8,9},{9,8},{10,11... | collective-permute-start | bytes 491528 | tf_op jit(solution)/shard_map/ppermute | solution.py:407
  62.2 19.3 %collective-permute-start.21 = (bf16[320,1024]{1,0:T(8,128)(2,1)S(1)}, bf16[320,1024]{1,0:T(8,128)(2,1)S(1)}, u32[]{:S(2)}, u32[]{:S(2)}) collective-permute-start(bf16[320,1024]{1,0:T(8,128)(2,1)S(1)} %get-tuple-element.100), channel_id=1, source_target_pairs={{0,1},{1,0},{2,3},{3,2},{4,5},{5,4},{6,7},{7,6},{8,9},{9,8},{10,11... | collective-permute-start | bytes 1966088 | tf_op jit(solution)/shard_map/ppermute | solution.py:407
  65.1 20.6 %collective-permute-start.26 = (bf16[320,1024]{1,0:T(8,128)(2,1)S(1)}, bf16[320,1024]{1,0:T(8,128)(2,1)S(1)}, u32[]{:S(2)}, u32[]{:S(2)}) collective-permute-start(bf16[320,1024]{1,0:T(8,128)(2,1)S(1)} %get-tuple-element.109), channel_id=1, source_target_pairs={{0,1},{1,0},{2,3},{3,2},{4,5},{5,4},{6,7},{7,6},{8,9},{9,8},{10,11... | collective-permute-start | bytes 1966088 | tf_op jit(solution)/shard_map/ppermute | solution.py:407
  65.3 6.0 %collective-permute-start.1 = (bf16[544,128]{1,0:T(8,128)(2,1)S(1)}, bf16[544,128]{1,0:T(8,128)(2,1)S(1)}, u32[]{:S(2)}, u32[]{:S(2)}) collective-permute-start(bf16[544,128]{1,0:T(8,128)(2,1)S(1)} %get-tuple-element.74), channel_id=1, source_target_pairs={{0,4},{4,0},{8,12},{12,8},{16,20},{20,16},{24,28},{28,24},{1,5},{5... | collective-permute-start | bytes 417800 | tf_op jit(solution)/shard_map/ppermute | solution.py:407
  71.9 5.4 %collective-permute-start.2 = (bf16[544,128]{1,0:T(8,128)(2,1)S(1)}, bf16[544,128]{1,0:T(8,128)(2,1)S(1)}, u32[]{:S(2)}, u32[]{:S(2)}) collective-permute-start(bf16[544,128]{1,0:T(8,128)(2,1)S(1)} %sp.1.mine_ref), channel_id=1, source_target_pairs={{0,8},{4,12},{8,0},{12,4},{16,24},{20,28},{24,16},{28,20},{1,9},{5... | collective-permute-start | bytes 417800 | tf_op jit(solution)/shard_map/ppermute | solution.py:407
  77.9 10.1 %collective-permute-start.3 = (bf16[544,128]{1,0:T(8,128)(2,1)S(1)}, bf16[544,128]{1,0:T(8,128)(2,1)S(1)}, u32[]{:S(2)}, u32[]{:S(2)}) collective-permute-start(bf16[544,128]{1,0:T(8,128)(2,1)S(1)} %get-tuple-element.77), channel_id=1, source_target_pairs={{0,16},{4,20},{8,24},{12,28},{1,17},{5,21},{9,25},{13,29},{2,18},{... | collective-permute-start | bytes 417800 | tf_op jit(solution)/shard_map/ppermute | solution.py:776
  82.2 7.0 %collective-permute-start.22 = (bf16[80,1024]{1,0:T(8,128)(2,1)S(1)}, bf16[80,1024]{1,0:T(8,128)(2,1)S(1)}, u32[]{:S(2)}, u32[]{:S(2)}) collective-permute-start(bf16[80,1024]{1,0:T(8,128)(2,1)S(1)} %get-tuple-element.102), channel_id=1, source_target_pairs={{0,4},{4,0},{8,12},{12,8},{16,20},{20,16},{24,28},{28,24},{1,5},{5... | collective-permute-start | bytes 491528 | tf_op jit(solution)/shard_map/ppermute | solution.py:407
  83.7 7.2 %collective-permute-start.23 = (bf16[80,1024]{1,0:T(8,128)(2,1)S(1)}, bf16[80,1024]{1,0:T(8,128)(2,1)S(1)}, u32[]{:S(2)}, u32[]{:S(2)}) collective-permute-start(bf16[80,1024]{1,0:T(8,128)(2,1)S(1)} %get-tuple-element.103), channel_id=1, source_target_pairs={{0,8},{4,12},{8,0},{12,4},{16,24},{20,28},{24,16},{28,20},{1,9},{5... | collective-permute-start | bytes 491528 | tf_op jit(solution)/shard_map/ppermute | solution.py:407
  85.4 6.7 %collective-permute-start.24 = (bf16[80,1024]{1,0:T(8,128)(2,1)S(1)}, bf16[80,1024]{1,0:T(8,128)(2,1)S(1)}, u32[]{:S(2)}, u32[]{:S(2)}) collective-permute-start(bf16[80,1024]{1,0:T(8,128)(2,1)S(1)} %get-tuple-element.104), channel_id=1, source_target_pairs={{0,12},{4,8},{8,4},{12,0},{16,28},{20,24},{24,20},{28,16},{1,13},{... | collective-permute-start | bytes 491528 | tf_op jit(solution)/shard_map/ppermute | solution.py:407
  86.4 8.5 %collective-permute-start.27 = (bf16[160,512]{1,0:T(8,128)(2,1)S(1)}, bf16[160,512]{1,0:T(8,128)(2,1)S(1)}, u32[]{:S(2)}, u32[]{:S(2)}) collective-permute-start(bf16[160,512]{1,0:T(8,128)(2,1)S(1)} %get-tuple-element.111), channel_id=1, source_target_pairs={{0,2},{1,3},{2,0},{3,1},{4,6},{5,7},{6,4},{7,5},{8,10},{9,11},{10,... | collective-permute-start | bytes 491528 | tf_op jit(solution)/shard_map/ppermute | solution.py:407
  88.0 11.1 %collective-permute-start.30 = (bf16[160,512]{1,0:T(8,128)(2,1)S(1)}, bf16[160,512]{1,0:T(8,128)(2,1)S(1)}, u32[]{:S(2)}, u32[]{:S(2)}) collective-permute-start(bf16[160,512]{1,0:T(8,128)(2,1)S(1)} %get-tuple-element.115), channel_id=1, source_target_pairs={{0,2},{1,3},{2,0},{3,1},{4,6},{5,7},{6,4},{7,5},{8,10},{9,11},{10,... | collective-permute-start | bytes 491528 | tf_op jit(solution)/shard_map/ppermute | solution.py:407
  89.2 14.0 %collective-permute-start.4 = (bf16[512,128]{1,0:T(8,128)(2,1)S(1)}, bf16[512,128]{1,0:T(8,128)(2,1)S(1)}, u32[]{:S(2)}, u32[]{:S(2)}) collective-permute-start(bf16[512,128]{1,0:T(8,128)(2,1)S(1)} %get-tuple-element.79), channel_id=1, source_target_pairs={{0,4},{4,0},{8,12},{12,8},{16,20},{20,16},{24,28},{28,24},{1,5},{5... | collective-permute-start | bytes 393224 | tf_op jit(solution)/shard_map/ppermute | solution.py:407
  93.4 17.1 %collective-permute-start.25 = (bf16[160,512]{1,0:T(8,128)(2,1)S(1)}, bf16[160,512]{1,0:T(8,128)(2,1)S(1)}, u32[]{:S(2)}, u32[]{:S(2)}) collective-permute-start(bf16[160,512]{1,0:T(8,128)(2,1)S(1)} %get-tuple-element.106), channel_id=1, source_target_pairs={{0,2},{1,3},{2,0},{3,1},{4,6},{5,7},{6,4},{7,5},{8,10},{9,11},{10,... | collective-permute-start | bytes 491528 | tf_op jit(solution)/shard_map/ppermute | solution.py:407
  95.5 12.3 %collective-permute-start.28 = (bf16[80,512]{1,0:T(8,128)(2,1)S(1)}, bf16[80,512]{1,0:T(8,128)(2,1)S(1)}, u32[]{:S(2)}, u32[]{:S(2)}) collective-permute-start(bf16[80,512]{1,0:T(8,128)(2,1)S(1)} %get-tuple-element.112), channel_id=1, source_target_pairs={{0,16},{4,20},{8,24},{12,28},{16,0},{20,4},{24,8},{28,12},{1,17},{... | collective-permute-start | bytes 245768 | tf_op jit(solution)/shard_map/ppermute | solution.py:407
  96.7 12.4 %collective-permute-start.29 = (bf16[80,512]{1,0:T(8,128)(2,1)S(1)}, bf16[80,512]{1,0:T(8,128)(2,1)S(1)}, u32[]{:S(2)}, u32[]{:S(2)}) collective-permute-start(bf16[80,512]{1,0:T(8,128)(2,1)S(1)} %get-tuple-element.113), channel_id=1, source_target_pairs={{0,20},{4,16},{8,28},{12,24},{16,4},{20,0},{24,12},{28,8},{1,21},{... | collective-permute-start | bytes 245768 | tf_op jit(solution)/shard_map/ppermute | solution.py:407
  99.7 9.4 %collective-permute-start.31 = (bf16[80,512]{1,0:T(8,128)(2,1)S(1)}, bf16[80,512]{1,0:T(8,128)(2,1)S(1)}, u32[]{:S(2)}, u32[]{:S(2)}) collective-permute-start(bf16[80,512]{1,0:T(8,128)(2,1)S(1)} %get-tuple-element.116), channel_id=1, source_target_pairs={{0,24},{4,28},{8,16},{12,20},{16,8},{20,12},{24,0},{28,4},{1,25},{... | collective-permute-start | bytes 245768 | tf_op jit(solution)/shard_map/ppermute | solution.py:407
  103.2 7.2 %collective-permute-start.32 = (bf16[80,512]{1,0:T(8,128)(2,1)S(1)}, bf16[80,512]{1,0:T(8,128)(2,1)S(1)}, u32[]{:S(2)}, u32[]{:S(2)}) collective-permute-start(bf16[80,512]{1,0:T(8,128)(2,1)S(1)} %get-tuple-element.117), channel_id=1, source_target_pairs={{0,28},{4,24},{8,20},{12,16},{16,12},{20,8},{24,4},{28,0},{1,29},{... | collective-permute-start | bytes 245768 | tf_op jit(solution)/shard_map/ppermute | solution.py:407
  (1 other events, 5.0 us)
